TPU v7x, 32 devices: a whole 2x2x4 slice. The times are simulated.
32 devices in a mesh: sp: 8 (over z, y), tp: 4 (over x, core).
Axes of the slice: x: 2, y: 2, z: 4, core: 2. Of those that a mesh axis runs over, the one named last changes fastest.
Arguments:
- conv_outer: bfloat16 [6144, 2048], P('sp', 'tp'), may hold values from -6 to 6
- conv_inner: bfloat16 [6144, 2048], P('sp', 'tp'), may hold values from -6 to 6
- conv_input: bfloat16 [6144, 2048], P('sp', 'tp'), may hold values from -6 to 6
- conv_taps: float32 [3, 2048], P(None, 'tp'), may hold values from -3.5 to 3.5
- out_weight: bfloat16 [2048, 2048], P('tp'), may hold values from -0.125 to 0.125
- mix_gate: bfloat16 [6144, 2048], P(('sp', 'tp')), may hold values from -8 to 8
- residual: bfloat16 [6144, 2048], P(('sp', 'tp')), may hold values from -6 to 6
- mix_gain: float32 [2048], replicated, may hold values from 0.1 to 1.9
- expert_gain: float32 [2048], replicated, may hold values from 0.1 to 1.9
- expert_ids: int32 [6144, 2], P(('sp', 'tp')), may hold values from 0 to 7, all different within a row; in each aligned block of 192 rows (0 to 191, 192 to 383, ...) at most 96 rows name the same one
- group_share: float32 [6144], P(('sp', 'tp')), may hold values from 0.25 to 1
- pair_scores: float32 [6144, 2], P(('sp', 'tp')), may hold values from -8 to 8
- gate_experts: bfloat16 [8, 2048, 512], P('sp'), may hold values from -0.125 to 0.125
- up_experts: bfloat16 [8, 2048, 512], P('sp'), may hold values from -0.125 to 0.125
- down_experts: bfloat16 [8, 512, 2048], P('sp'), may hold values from -0.25 to 0.25
Outputs:
- layer_out: bfloat16 [6144, 2048], P(('sp', 'tp'))
Inputs may be any that keep to these rules, and one draw needn't show every extreme that they name: `expert_ids`: within the rows of one device (aligned blocks of 192 rows), no expert is named by more than 96 rows, a bound that some block reaches; the 2 experts of a row differ.
All inputs are finite; a program needn't handle non-finite values.
Results may differ from a plain program's by a relative error of at most 0.0069.
Values may be sent and summed in bfloat16 or wider, within the bound.
A program may use at most 128 MiB of HBM per device.

v0:
```python
import jax
import jax.numpy as jnp
from jax import lax
from jax.experimental import pallas as pl
from jax.experimental.pallas import tpu as pltpu
from jax.sharding import PartitionSpec as P

epsilon = 1e-06


def f32(value):
    return value.astype(jnp.float32)


def bf16(value):
    return value.astype(jnp.bfloat16)


def rms_scale(values, gain):
    return values * lax.rsqrt(jnp.mean(values * values, axis=-1, keepdims=True) + epsilon) * gain


def shifted(value, steps, senders):
    return lax.ppermute(value, "sp", [(s, s + steps) for s in senders])


def swapped(value, axis, bit):
    return lax.ppermute(value, axis, [(s, s ^ bit) for s in range(lax.axis_size(axis))])


def mixer_rows(conv_outer, conv_inner, conv_input, conv_taps):
    kept = conv_taps.shape[0] - 1
    inner = f32(conv_inner) * f32(conv_input)
    tail = f32(conv_inner[-kept:]) * f32(conv_input[-kept:])
    earlier = shifted(tail, 1, range(lax.axis_size("sp") - 1))
    length = conv_inner.shape[0]
    inner = jnp.concatenate([earlier, inner], 0)
    conv = conv_taps[0] * inner[0:length]
    for offset in range(1, kept + 1):
        conv = conv + conv_taps[offset] * inner[offset : offset + length]
    return bf16(f32(conv_outer) * conv)


def project(mixed_rows, out_weight, own_rows):
    parts = lax.axis_size("tp")
    me = lax.axis_index("tp")
    blocks = mixed_rows.reshape(parts, own_rows, -1)

    def partial(owner):
        rows = lax.dynamic_index_in_dim(blocks, owner, 0, keepdims=False)
        return jnp.dot(rows, out_weight, preferred_element_type=jnp.float32)

    def total(owner_bits, bit):
        if bit == 1:
            return partial(me ^ owner_bits)
        half = bit // 2
        sent = bf16(total(owner_bits | half, half))
        given = swapped(sent, "tp", half)
        return total(owner_bits, half) + f32(given)

    return total(0, parts)


def routing_table(expert_ids, group_share, pair_scores, own_rows, count):
    weights = group_share[:, None] * jax.nn.softmax(pair_scores, axis=-1)
    lanes = -(-2 * count // 128) * 128
    column = jnp.arange(lanes, dtype=jnp.int32)[None, :]
    coarse = lax.reduce_precision(weights, 8, 7)
    fine = weights - coarse
    table = jnp.zeros((own_rows, lanes), jnp.float32)
    for slot in range(expert_ids.shape[1]):
        at = expert_ids[:, slot : slot + 1]
        table = table + jnp.where(column == at, coarse[:, slot : slot + 1], 0.0)
        table = table + jnp.where(column == at + count, fine[:, slot : slot + 1], 0.0)
    return bf16(table)


def per_device(
    conv_outer,
    conv_inner,
    conv_input,
    conv_taps,
    out_weight,
    mix_gate,
    residual,
    mix_gain,
    expert_gain,
    expert_ids,
    group_share,
    pair_scores,
    gate_experts,
    up_experts,
    down_experts,
):
    count = lax.axis_size("sp")
    me = lax.axis_index("sp")
    own_rows = residual.shape[0]
    groups = count // 2
    place = me // 2
    side = lax.axis_index("tp") % 2
    half = gate_experts.shape[2] // 2

    def fetched(weight, axis):
        piece = lax.dynamic_slice_in_dim(weight[0], side * half, half, axis)
        first = swapped(piece, "sp", 1)
        second = swapped(first, "tp", 1)
        return jnp.concatenate([weight[0], first, second], axis)

    gate_both = fetched(gate_experts, 1)
    up_both = fetched(up_experts, 1)
    down_both = fetched(down_experts, 0)

    lanes = -(-2 * count // 128) * 128
    table = routing_table(expert_ids, group_share, pair_scores, own_rows, count)

    def spread(own):
        below, above = {0: own}, {0: own}
        for step in range(1, groups):
            below[step] = shifted(below[step - 1], 2, range(2 * (step - 1), count - 2))
            above[step] = shifted(above[step - 1], -2, range(2, count - 2 * (step - 1)))
        order = {0: own}
        for near in range(1, (groups - 1) // 2 + 1):
            far = groups - near
            early = jnp.where(place < near, above[near], below[near])
            _, over, under, away = lax.optimization_barrier(
                (early, above[near], below[far], above[far])
            )
            order[near] = early
            late = jnp.where(place < far, over, under)
            order[far] = jnp.where(place < near, away, late)
        if groups % 2 == 0:
            mid = groups // 2
            order[mid] = jnp.where(place < mid, above[mid], below[mid])
        return order

    mixed_rows = mixer_rows(conv_outer, conv_inner, conv_input, conv_taps)
    projected = project(mixed_rows, out_weight, own_rows)
    mixed = jax.nn.sigmoid(f32(mix_gate)) * projected
    hidden_state = bf16(f32(residual) + rms_scale(mixed, mix_gain))
    normed = bf16(rms_scale(f32(hidden_state), expert_gain))

    blocks = spread(jnp.concatenate([normed, table], 1))
    depth = normed.shape[1]

    def served(block):
        rows = block[:, :depth]
        chosen = jnp.arange(lanes, dtype=jnp.int32)[:, None] % count
        picks = bf16(chosen == jnp.stack([me, me ^ 1])[None, :])
        picks = jnp.where(jnp.arange(lanes)[:, None] < 2 * count, picks, 0)
        shares = jnp.dot(block[:, depth:], picks, preferred_element_type=jnp.float32)
        wide = 2 * half
        first = jnp.dot(rows, gate_both, preferred_element_type=jnp.float32)
        second = jnp.dot(rows, up_both, preferred_element_type=jnp.float32)
        mine = jnp.arange(2 * wide)[None, :] < wide
        share = jnp.where(mine, shares[:, :1], shares[:, 1:])
        hidden = lax.optimization_barrier(bf16(jax.nn.silu(first) * second * share))
        return lax.optimization_barrier(
            jnp.dot(hidden, down_both, preferred_element_type=jnp.float32)
        )

    results = {number: served(block) for number, block in blocks.items()}

    def for_upper(step):
        gone = groups - step
        if step == gone or step < gone:
            return results[gone]
        return jnp.where(place < gone, results[gone], results[step])

    down = up = None
    for step in range(1, groups):
        gone = groups - step
        lower, upper = results[gone], for_upper(step)
        if down is not None:
            lower, upper = lower + f32(down), upper + f32(up)
        down = shifted(bf16(lower), -2, range(2 * gone, count))
        up = shifted(bf16(upper), 2, range(0, count - 2 * gone))
    result = f32(hidden_state) + results[0]
    if down is not None:
        result = result + f32(down) + f32(up)
    return bf16(result)


MESH_ID = pl.DeviceIdType.MESH
OWN, OTHER, OUT, ARRIVE, FORWARD = 8, 16, 32, 64, 128

OUTER_STEPS = (
    0 | OWN,
    1 | OWN,
    2 | OWN | ARRIVE,
    4 | OWN | ARRIVE,
    0,
    0,
    4 | OTHER | OUT,
    2 | OTHER,
    6 | OWN | OTHER | OUT | ARRIVE,
    0 | OTHER,
    7 | OWN | OTHER | OUT | ARRIVE,
    1 | OTHER,
    5 | OWN | OTHER | OUT | ARRIVE,
    2 | OUT,
    3 | OWN | OTHER | OUT | ARRIVE,
    0 | OUT,
    1 | OUT,
    0,
    0,
    0,
    0,
    0,
)
INNER_STEPS = (
    2 | OWN,
    3 | OWN,
    0 | OWN | ARRIVE | FORWARD,
    4 | OWN | ARRIVE | FORWARD,
    1 | OWN | ARRIVE | FORWARD,
    6 | OWN | ARRIVE | FORWARD,
    4 | OTHER,
    6 | OTHER,
    7 | OWN | OTHER | ARRIVE | FORWARD,
    4 | OUT,
    5 | OWN | OTHER | ARRIVE | FORWARD,
    6 | OUT,
    1 | OTHER,
    0 | OTHER,
    7 | OUT,
    0 | OUT,
    2 | OTHER,
    5 | OUT,
    1 | OUT,
    3 | OTHER,
    2 | OUT,
    3 | OUT,
)
WEIGHTS_STEP = 6
LATE_ACROSS = 4
LATE_OUTWARD = 10


def mega_kernel(
    co_hbm, ci_hbm, cx_hbm, taps, ow_hbm, mg_hbm, res_hbm, mgain, egain, table_hbm,
    g_hbm, u_hbm, d_hbm, out_hbm,
    ci, cx, co, ow, mg, res, mix, acc, part_out, part_in, x_out, x_in,
    X, T, P, S, H, g1, u1, g2, u2, wd, picks,
    load_sem, halo_s, halo_r, tab_s, tab_r, core_s, core_r, xsw_s, xsw_r,
    w_s, w_r, rows_s, rows_r, sum_s, sum_r, out_sem,
):
    sp = lax.axis_index("sp")
    tp = lax.axis_index("tp")
    z = sp // 2
    y = sp % 2
    half = z // 2
    outer = z * (3 - z) == 0
    inner = jnp.logical_not(outer)
    own = jnp.where(outer, 0, 1)
    core_peer = tp + 1 - 2 * (tp % 2)
    x_peer = (tp + 2) % 4
    y_peer = sp + 1 - 2 * y
    rows, depth = res.shape
    piece = rows // 2
    width = g1.shape[1]
    count = 8
    channels = ow.shape[0]
    halo = ci.shape[0] - co.shape[0]

    def line(slot):
        where = jnp.where(slot == 0, 3 * half, jnp.where(slot == 1, 1 + half, jnp.where(slot == 2, 2 - half, 3 - 3 * half)))
        return 2 * where + y

    def remote(src, dst, s, r, device):
        return pltpu.make_async_remote_copy(
            src_ref=src, dst_ref=dst, send_sem=s, recv_sem=r, device_id=device, device_id_type=MESH_ID
        )

    tokens = co.shape[0]
    loads = [
        pltpu.make_async_copy(ci_hbm, ci.at[pl.ds(halo, tokens)], load_sem.at[0]),
        pltpu.make_async_copy(cx_hbm, cx.at[pl.ds(halo, tokens)], load_sem.at[1]),
        pltpu.make_async_copy(co_hbm, co, load_sem.at[2]),
        pltpu.make_async_copy(ow_hbm, ow, load_sem.at[3]),
        pltpu.make_async_copy(mg_hbm, mg, load_sem.at[4]),
        pltpu.make_async_copy(res_hbm, res, load_sem.at[5]),
        pltpu.make_async_copy(g_hbm.at[0], g1, load_sem.at[6]),
        pltpu.make_async_copy(u_hbm.at[0], u1, load_sem.at[7]),
        pltpu.make_async_copy(d_hbm.at[0], wd.at[pl.ds(0, width)], load_sem.at[8]),
        pltpu.make_async_copy(table_hbm, T.at[pl.ds(2 * own, 2)], load_sem.at[9]),
    ]
    for copy in loads:
        copy.start()

    barrier = pltpu.get_barrier_semaphore()

    def greet(device):
        pl.semaphore_signal(barrier, inc=1, device_id=device, device_id_type=MESH_ID)

    greet((sp, core_peer))
    greet((sp, x_peer))
    greet((y_peer, tp))
    for away in range(1, 4):
        greet(((sp + 2 * away) % count, tp))
    has_next = jnp.logical_and(y == 1, sp < count - 1)
    has_last = jnp.logical_and(y == 0, sp > 0)

    @pl.when(has_next)
    def _():
        greet((sp + 1, tp))

    @pl.when(has_last)
    def _():
        greet((sp - 1, tp))

    pl.semaphore_wait(barrier, 6 + jnp.where(has_next, 1, 0) + jnp.where(has_last, 1, 0))

    def halo_copy(k, device):
        src = (ci_hbm, cx_hbm)[k].at[pl.ds(tokens - halo, halo)]
        return remote(src, (ci, cx)[k].at[pl.ds(0, halo)], halo_s.at[k], halo_r.at[k], device)

    @pl.when(sp < count - 1)
    def _():
        for k in range(2):
            halo_copy(k, (sp + 1, tp)).start()

    quarter = depth // 4
    wide = width // 2
    mine = pl.multiple_of(tp * quarter, quarter)
    theirs = pl.multiple_of(x_peer * quarter, quarter)
    side = tp % 2

    def weight_copy(k, leg):
        at = 4 * k + leg
        if k < 2:
            buf = (g2, u2)[k]
            rows_at = pl.ds(theirs if leg == 3 else mine, quarter)
            src = (g_hbm, u_hbm)[k].at[0, rows_at] if leg == 0 else buf.at[rows_at]
            dst = buf.at[rows_at]
        else:
            rows_at = pl.ds(pl.multiple_of(width + side * wide, wide), wide)
            src = d_hbm.at[0, pl.ds(pl.multiple_of(side * wide, wide), wide)] if leg == 0 else wd.at[rows_at]
            dst = wd.at[rows_at]
        device = ((y_peer, tp), (sp, core_peer), (sp, x_peer), (sp, core_peer))[leg]
        return remote(src, dst, w_s.at[at], w_r.at[at], device)

    for k in range(3):
        weight_copy(k, 0).start()

    def table_copy(away):
        zz = (z + away) % 4
        same = zz // 2 == half
        slot = jnp.where(same, own, 3 - own)
        return remote(
            table_hbm, T.at[pl.ds(2 * slot, 2)], tab_s.at[away], tab_r.at[slot], ((sp + 2 * away) % count, tp)
        )

    for away in range(1, 4):
        table_copy(away).start()

    P[0] = jnp.zeros(P.shape[1:], P.dtype)
    lane = lax.broadcasted_iota(jnp.int32, (T.shape[2], width), 0)
    for k in range(2):
        expert = (sp, y_peer)[k]
        picks[k] = jnp.where(jnp.logical_and(lane % count == expert, lane < 2 * count), 1.0, 0.0).astype(picks.dtype)

    for k in range(3):
        loads[k].wait()

    @pl.when(sp == 0)
    def _():
        ci[pl.ds(0, halo)] = jnp.zeros((halo, channels), ci.dtype)
        cx[pl.ds(0, halo)] = jnp.zeros((halo, channels), cx.dtype)

    @pl.when(sp > 0)
    def _():
        for k in range(2):
            halo_copy(k, (sp, core_peer)).wait_recv()

    kept = taps.shape[0] - 1
    run = 32

    def conv(block):
        def some(i, c):
            at = pl.multiple_of(block * rows + i * run, run)
            near = f32(ci[pl.ds(at, halo + run)]) * f32(cx[pl.ds(at, halo + run)])
            total = taps[0:1] * near[halo - kept : halo - kept + run]
            for j in range(1, kept + 1):
                total = total + taps[j : j + 1] * near[halo - kept + j : halo - kept + j + run]
            mix[pl.ds(at, run)] = bf16(f32(co[pl.ds(at, run)]) * total)
            return c

        lax.fori_loop(0, rows // run, some, 0)

    tile = min(512, depth)
    loads[3].wait()

    def core_copy(k):
        return remote(part_out.at[k], part_in.at[k], core_s.at[k], core_r.at[k], (sp, core_peer))

    def x_copy(c):
        return remote(x_out.at[c], x_in.at[c], xsw_s.at[c], xsw_r.at[c], (sp, x_peer))

    def projected(i, carry):
        owner = jnp.where(i == 0, 3 - tp, jnp.where(i == 1, x_peer, jnp.where(i == 2, core_peer, tp)))
        conv(owner)

        def some(n, c):
            cols = pl.ds(pl.multiple_of(n * tile, tile), tile)
            got = jnp.dot(
                mix[pl.ds(pl.multiple_of(owner * rows, rows), rows)], ow[:, cols], preferred_element_type=jnp.float32
            )

            @pl.when(i % 2 == 0)
            def _():
                part_out[i // 2, :, cols] = bf16(got)

            @pl.when(i % 2 == 1)
            def _():
                acc[:, cols] = got

            return c

        lax.fori_loop(0, depth // tile, some, 0)

        @pl.when(i == 0)
        def _():
            core_copy(0).start()

        @pl.when(i == 1)
        def _():
            core_copy(0).wait_recv()

            def add(r, c):
                at = pl.ds(pl.multiple_of(r * 16, 16), 16)
                for k in range(2):
                    src = pl.ds(pl.multiple_of(k * piece + r * 16, 16), 16)
                    x_out[k, at] = bf16(acc[src] + f32(part_in[0, src]))
                return c

            lax.fori_loop(0, piece // 16, add, 0)
            x_copy(0).start()
            x_copy(1).start()

        @pl.when(i == 2)
        def _():
            core_copy(1).start()

        return carry

    lax.fori_loop(0, 4, projected, 0)
    core_copy(1).wait_recv()
    loads[4].wait()
    loads[5].wait()

    def rows_copy(item, device, dst, at):
        return remote(X.at[item], X.at[dst], rows_s.at[at], rows_r.at[dst], device)

    def normalize(c):
        def some(r, carry):
            at = pl.ds(pl.multiple_of(r * 16, 16), 16)
            src = pl.ds(pl.multiple_of(c * piece + r * 16, 16), 16)
            total = acc[src] + f32(part_in[1, src]) + f32(x_in[c, at])
            mixed = jax.nn.sigmoid(f32(mg[src])) * total
            state = bf16(f32(res[src]) + rms_scale(mixed, mgain[...]))
            P[1 + c, at] = state
            X[2 * own + c, at] = bf16(rms_scale(f32(state), egain[...]))
            return carry

        lax.fori_loop(0, piece // 16, some, 0)

    def send_own(c, across):
        item = 2 * own + c
        if across:
            rows_copy(item, (line(2), tp), 4 + c, 8 + c).start()
        else:
            rows_copy(item, (line(1 - own), tp), item, item).start()

    def relay(k, leg):
        weight_copy(k, leg).wait_recv()

    relay(0, 0)
    weight_copy(0, 1).start()
    weight_copy(0, 2).start()
    x_copy(0).wait_recv()
    normalize(0)
    send_own(0, False)

    @pl.when(inner)
    def _():
        send_own(0, True)

    x_copy(1).wait_recv()
    normalize(1)

    @pl.when(outer)
    def _():
        send_own(1, False)

    relay(1, 0)
    weight_copy(1, 1).start()
    weight_copy(1, 2).start()
    for k in range(6, 10):
        loads[k].wait()
    for away in range(1, 4):
        slot = (own + away) % 4
        remote(table_hbm, T.at[pl.ds(2 * slot, 2)], tab_s.at[away], tab_r.at[slot], (sp, core_peer)).wait_recv()

    def hidden(item, k):
        gate, up = ((g1, u1), (g2, u2))[k]
        x = X[item]
        first = jnp.dot(x, gate[...], preferred_element_type=jnp.float32)
        second = jnp.dot(x, up[...], preferred_element_type=jnp.float32)
        share = jnp.dot(T[item], picks[k], preferred_element_type=jnp.float32)
        H[item, :, k * width : (k + 1) * width] = bf16(jax.nn.silu(first) * second * share)

    def sum_copy(item):
        slot = item // 2
        c = item % 2
        to = jnp.where(outer, 1, jnp.where(slot == 0, 0, 2))
        dst = jnp.where(
            outer, 1 + item, jnp.where(slot == 0, 9 + c, jnp.where(slot == 2, 11 + c, 9 + c))
        )
        return remote(S.at[item], P.at[dst], sum_s.at[item], sum_r.at[dst], (line(to), tp))

    def out_copy(c):
        return pltpu.make_async_copy(
            S.at[2 * own + c], out_hbm.at[pl.ds(pl.multiple_of(c * piece, piece), piece)], out_sem.at[c]
        )

    def came(at):
        remote(S.at[0], P.at[at], sum_s.at[0], sum_r.at[at], (sp, core_peer)).wait_recv()

    def step(n, carry):
        code = 0
        for i, (a, b) in enumerate(zip(OUTER_STEPS, INNER_STEPS)):
            code = jnp.where(n == i, jnp.where(outer, a, b), code)
        item = code % 8

        def has(flag):
            return code // flag % 2 == 1

        slot = item // 2
        c = item % 2

        @pl.when(has(ARRIVE))
        def _():
            rows_copy(item, (sp, core_peer), item, item).wait_recv()

        @pl.when(has(FORWARD))
        def _():
            across = slot == 0
            rows_copy(
                item,
                (line(jnp.where(across, 2, 0)), tp),
                jnp.where(across, 6 + c, item),
                jnp.where(across, 10 + c, item),
            ).start()

        @pl.when(jnp.logical_and(inner, n == LATE_ACROSS))
        def _():
            send_own(1, True)

        @pl.when(jnp.logical_and(inner, n == LATE_OUTWARD))
        def _():
            send_own(1, False)

        @pl.when(n == WEIGHTS_STEP)
        def _():
            relay(0, 2)
            weight_copy(0, 3).start()
            relay(1, 2)
            weight_copy(1, 3).start()
            relay(2, 0)
            weight_copy(2, 1).start()
            for k, leg in ((0, 1), (1, 1), (0, 3), (1, 3), (2, 1)):
                got = pl.multiple_of((core_peer if leg == 1 else 3 - tp) * quarter, quarter)
                if k < 2:
                    at = (g2, u2)[k].at[pl.ds(got, quarter)]
                else:
                    at = wd.at[pl.ds(pl.multiple_of(width + (1 - side) * wide, wide), wide)]
                remote(at, at, w_s.at[4 * k + leg], w_r.at[4 * k + leg], (sp, core_peer)).wait_recv()

        @pl.when(has(OWN))
        def _():
            hidden(item, 0)

        @pl.when(has(OTHER))
        def _():
            hidden(item, 1)

        @pl.when(has(OUT))
        def _():
            a = jnp.where(slot == 0, 9 + c, jnp.where(outer, 0, 1 + item))
            b = jnp.where(outer, 0, jnp.where(slot == 1, 11 + c, 0))
            d = jnp.where(slot == own, 1 + c, 0)

            @pl.when(a > 0)
            def _():
                came(a)

            @pl.when(b > 0)
            def _():
                came(b)

            def some(m, carry):
                cols = pl.ds(pl.multiple_of(m * tile, tile), tile)
                got = jnp.dot(H[item], wd[:, cols], preferred_element_type=jnp.float32)
                got = got + f32(P[d, :, cols]) + f32(P[a, :, cols]) + f32(P[b, :, cols])
                S[item, :, cols] = bf16(got)
                return carry

            lax.fori_loop(0, depth // tile, some, 0)

            @pl.when(slot == own)
            def _():
                out_copy(c).start()

            @pl.when(slot != own)
            def _():
                sum_copy(item).start()

        return carry

    lax.fori_loop(0, len(OUTER_STEPS), step, 0)

    for c in range(2):
        out_copy(c).wait()
        core_copy(c).wait_send()
        x_copy(c).wait_send()

    @pl.when(sp < count - 1)
    def _():
        for k in range(2):
            halo_copy(k, (sp + 1, tp)).wait_send()

    for k in range(3):
        for leg in range(4 if k < 2 else 2):
            weight_copy(k, leg).wait_send()
    for away in range(1, 4):
        table_copy(away).wait_send()

    def gone(item, at):
        rows_copy(item, (sp, core_peer), item, at).wait_send()

    for c in range(2):
        gone(2 * own + c, 2 * own + c)
    for i in range(3):
        for c in range(2):
            item = 2 * ((own + 1 + i) % 4) + c
            remote(S.at[item], P.at[0], sum_s.at[item], sum_r.at[0], (sp, core_peer)).wait_send()

    @pl.when(inner)
    def _():
        for c in range(2):
            for at in (4 + c, 6 + c, 8 + c, 10 + c):
                gone(at % 8, at)


def mega(
    conv_outer, conv_inner, conv_input, conv_taps, out_weight, mix_gate, residual, mix_gain, expert_gain,
    expert_ids, group_share, pair_scores, gate_experts, up_experts, down_experts,
):
    count = lax.axis_size("sp")
    rows, depth = residual.shape
    tokens, channels = conv_inner.shape
    width = gate_experts.shape[2]
    piece = rows // 2
    table = routing_table(expert_ids, group_share, pair_scores, rows, count)
    lanes = table.shape[1]
    table = table.reshape(2, piece, lanes)
    halo = 16
    half_type, full = jnp.bfloat16, jnp.float32
    hbm = pl.BlockSpec(memory_space=pl.ANY)
    vmem = pl.BlockSpec(memory_space=pltpu.VMEM)
    dma = pltpu.SemaphoreType.DMA
    return pl.pallas_call(
        mega_kernel,
        out_shape=jax.ShapeDtypeStruct((rows, depth), half_type),
        in_specs=[hbm, hbm, hbm, vmem, hbm, hbm, hbm, vmem, vmem, hbm, hbm, hbm, hbm],
        out_specs=hbm,
        scratch_shapes=[
            pltpu.VMEM((halo + tokens, channels), half_type),
            pltpu.VMEM((halo + tokens, channels), half_type),
            pltpu.VMEM((tokens, channels), half_type),
            pltpu.VMEM((channels, depth), half_type),
            pltpu.VMEM((rows, depth), half_type),
            pltpu.VMEM((rows, depth), half_type),
            pltpu.VMEM((tokens, channels), half_type),
            pltpu.VMEM((rows, depth), full),
            pltpu.VMEM((2, rows, depth), half_type),
            pltpu.VMEM((2, rows, depth), half_type),
            pltpu.VMEM((2, piece, depth), half_type),
            pltpu.VMEM((2, piece, depth), half_type),
            pltpu.VMEM((8, piece, depth), half_type),
            pltpu.VMEM((8, piece, lanes), half_type),
            pltpu.VMEM((13, piece, depth), half_type),
            pltpu.VMEM((8, piece, depth), half_type),
            pltpu.VMEM((8, piece, 2 * width), half_type),
            pltpu.VMEM((depth, width), half_type),
            pltpu.VMEM((depth, width), half_type),
            pltpu.VMEM((depth, width), half_type),
            pltpu.VMEM((depth, width), half_type),
            pltpu.VMEM((2 * width, depth), half_type),
            pltpu.VMEM((2, lanes, width), half_type),
            dma((10,)),
            dma((2,)),
            dma((2,)),
            dma((4,)),
            dma((4,)),
            dma((2,)),
            dma((2,)),
            dma((2,)),
            dma((2,)),
            dma((12,)),
            dma((12,)),
            dma((16,)),
            dma((8,)),
            dma((8,)),
            dma((13,)),
            dma((2,)),
        ],
        compiler_params=pltpu.CompilerParams(
            collective_id=0, has_side_effects=True, vmem_limit_bytes=60 * 1024 * 1024
        ),
        name="layer",
    )(
        conv_outer, conv_inner, conv_input, conv_taps, out_weight, mix_gate, residual,
        mix_gain[None, :], expert_gain[None, :], table, gate_experts, up_experts, down_experts,
    )


def solution(mesh):
    placed = (
        P("sp", "tp"),
        P("sp", "tp"),
        P("sp", "tp"),
        P(None, "tp"),
        P("tp", None),
        P(("sp", "tp"), None),
        P(("sp", "tp"), None),
        P(),
        P(),
        P(("sp", "tp"), None),
        P(("sp", "tp")),
        P(("sp", "tp"), None),
        P("sp", None, None),
        P("sp", None, None),
        P("sp", None, None),
    )

    square = mesh.shape["tp"] == 4 and mesh.shape["sp"] == 8

    def layer(*arrays):
        return (mega if square else per_device)(*arrays)

    return jax.shard_map(
        layer, mesh=mesh, in_specs=placed, out_specs=P(("sp", "tp"), None), check_vma=False
    )
```

profile of v0, /device:TPU:12, one launch (start us, length us, event | category | flops | bytes accessed | tf_op | source)
XLA Modules:
  0.0 119.6 jit_solution(10101279865419102285)
XLA Ops:
  0.0 0.7 reduce_max.9
  0.7 0.7 fusion
  1.4 0.7 fusion.1
  2.2 0.1 broadcast_in_dim.53
  2.2 0.1 broadcast_in_dim.57
  2.3 0.1 broadcast_in_dim.55
  2.4 0.1 broadcast_in_dim.50
  2.5 0.8 slice_reduce_fusion.5
  3.3 0.1 eq.65
  3.3 0.1 eq.69
  3.4 0.1 eq.77
  3.5 0.1 eq.73
  3.6 0.9 add_convert_fusion.table_hbm
  4.5 113.0 %layer.1 = bf16[192,2048]{1,0:T(8,128)(2,1)} custom-call(bf16[768,512]{1,0:T(8,128)(2,1)} %co_hbm.1, bf16[768,512]{1,0:T(8,128)(2,1)} %ci_hbm.1, bf16[768,512]{1,0:T(8,128)(2,1)} %cx_hbm.1, f32[3,512]{1,0:T(4,128)} %taps.1, bf16[512,2048]{1,0:T(8,128)(2,1)} %ow_hbm.1, bf16[192,2048]{1,0:T(8,128)(2,1)} %mg_hbm.1, bf16[192,2048]{1,0:T(8,128)(2,1)} %res_hbm.1, ...), custom_call_target="tpu_custom_call" | custom-call | tf_op jit(solution)/shard_map/layer/pallas_call | solution.py:672
  117.5 2.1 %copy.17 = bf16[192,2048]{1,0:T(8,128)(2,1)} copy(bf16[192,2048]{1,0:T(8,128)(2,1)} %layer.1) | data formatting | bytes 1572864
  (2 shorter events, 0.0 us)
where the time goes:
time: 120 us
  Pallas kernels  113 us (94%)
  other arithmetic  3.78 us (3%)
  local copies, waits for them, and re-layouts  2.77 us (2%)
    pallas_call x1, Pallas kernels, mega(): pl.pallas_call(mega_kernel, out_shape=jax.ShapeDtypeStruct((rows, depth),...  113 us

commit v1 on v0

--- a/solution.py
+++ b/solution.py
@@ -237,7 +237,7 @@
 
 
 def mega_kernel(
-    co_hbm, ci_hbm, cx_hbm, taps, ow_hbm, mg_hbm, res_hbm, mgain, egain, table_hbm,
+    co_hbm, ci_hbm, cx_hbm, taps, ow_hbm, mg_hbm, res_hbm, mgain, egain, ids, scores, group,
     g_hbm, u_hbm, d_hbm, out_hbm,
     ci, cx, co, ow, mg, res, mix, acc, part_out, part_in, x_out, x_in,
     X, T, P, S, H, g1, u1, g2, u2, wd, picks,
@@ -258,7 +258,7 @@
     rows, depth = res.shape
     piece = rows // 2
     width = g1.shape[1]
-    count = 8
+    count = T.shape[1] // 2
     channels = ow.shape[0]
     halo = ci.shape[0] - co.shape[0]
 
@@ -282,10 +282,24 @@
         pltpu.make_async_copy(g_hbm.at[0], g1, load_sem.at[6]),
         pltpu.make_async_copy(u_hbm.at[0], u1, load_sem.at[7]),
         pltpu.make_async_copy(d_hbm.at[0], wd.at[pl.ds(0, width)], load_sem.at[8]),
-        pltpu.make_async_copy(table_hbm, T.at[pl.ds(2 * own, 2)], load_sem.at[9]),
     ]
-    for copy in loads:
-        copy.start()
+    for k in (0, 1, 3, 2):
+        loads[k].start()
+
+    raw = scores[...]
+    top = jnp.maximum(raw[0:1], raw[1:2])
+    up = jnp.exp(raw - top)
+    weights = group[...] * (up / (up[0:1] + up[1:2]))
+    coarse = f32(bf16(weights))
+    fine = weights - coarse
+    line_of = lax.broadcasted_iota(jnp.int32, (T.shape[1], rows), 0)
+    entries = jnp.zeros((T.shape[1], rows), jnp.float32)
+    for k in range(2):
+        entries = entries + jnp.where(line_of == ids[k : k + 1], coarse[k : k + 1], 0.0)
+        entries = entries + jnp.where(line_of == ids[k : k + 1] + count, fine[k : k + 1], 0.0)
+    entries = bf16(entries)
+    for p in range(2):
+        T[2 * own + p] = entries[:, (1 - p) * piece : (2 - p) * piece]
 
     barrier = pltpu.get_barrier_semaphore()
 
@@ -347,37 +361,32 @@
         same = zz // 2 == half
         slot = jnp.where(same, own, 3 - own)
         return remote(
-            table_hbm, T.at[pl.ds(2 * slot, 2)], tab_s.at[away], tab_r.at[slot], ((sp + 2 * away) % count, tp)
+            T.at[pl.ds(2 * own, 2)],
+            T.at[pl.ds(2 * slot, 2)],
+            tab_s.at[away],
+            tab_r.at[slot],
+            ((sp + 2 * away) % count, tp),
         )
 
     for away in range(1, 4):
         table_copy(away).start()
 
     P[0] = jnp.zeros(P.shape[1:], P.dtype)
-    lane = lax.broadcasted_iota(jnp.int32, (T.shape[2], width), 0)
+    lane = lax.broadcasted_iota(jnp.int32, (T.shape[1], width), 0)
     for k in range(2):
-        expert = (sp, y_peer)[k]
-        picks[k] = jnp.where(jnp.logical_and(lane % count == expert, lane < 2 * count), 1.0, 0.0).astype(picks.dtype)
+        picks[k] = jnp.where(lane % count == (sp, y_peer)[k], 1.0, 0.0).astype(picks.dtype)
 
     for k in range(3):
         loads[k].wait()
-
-    @pl.when(sp == 0)
-    def _():
-        ci[pl.ds(0, halo)] = jnp.zeros((halo, channels), ci.dtype)
-        cx[pl.ds(0, halo)] = jnp.zeros((halo, channels), cx.dtype)
-
-    @pl.when(sp > 0)
-    def _():
-        for k in range(2):
-            halo_copy(k, (sp, core_peer)).wait_recv()
+    for k in range(4, 9):
+        loads[k].start()
 
     kept = taps.shape[0] - 1
     run = 32
 
-    def conv(block):
+    def conv(start):
         def some(i, c):
-            at = pl.multiple_of(block * rows + i * run, run)
+            at = pl.multiple_of(start + i * run, run)
             near = f32(ci[pl.ds(at, halo + run)]) * f32(cx[pl.ds(at, halo + run)])
             total = taps[0:1] * near[halo - kept : halo - kept + run]
             for j in range(1, kept + 1):
@@ -385,66 +394,74 @@
             mix[pl.ds(at, run)] = bf16(f32(co[pl.ds(at, run)]) * total)
             return c
 
-        lax.fori_loop(0, rows // run, some, 0)
+        lax.fori_loop(0, piece // run, some, 0)
 
     tile = min(512, depth)
     loads[3].wait()
 
-    def core_copy(k):
-        return remote(part_out.at[k], part_in.at[k], core_s.at[k], core_r.at[k], (sp, core_peer))
-
-    def x_copy(c):
-        return remote(x_out.at[c], x_in.at[c], xsw_s.at[c], xsw_r.at[c], (sp, x_peer))
+    def core_copy(phase, p):
+        at = 2 * phase + p
+        return remote(part_out.at[at], part_in.at[at], core_s.at[at], core_r.at[at], (sp, core_peer))
+
+    def x_copy(p):
+        return remote(x_out.at[p], x_in.at[p], xsw_s.at[p], xsw_r.at[p], (sp, x_peer))
 
     def projected(i, carry):
-        owner = jnp.where(i == 0, 3 - tp, jnp.where(i == 1, x_peer, jnp.where(i == 2, core_peer, tp)))
-        conv(owner)
+        phase = i // 4
+        p = i // 2 % 2
+        second = i % 2 == 1
+        owner = jnp.where(
+            phase == 0, jnp.where(second, x_peer, 3 - tp), jnp.where(second, tp, core_peer)
+        )
+        start = pl.multiple_of(owner * rows + (1 - p) * piece, piece)
+
+        @pl.when(jnp.logical_and(i == 2, sp == 0))
+        def _():
+            ci[pl.ds(0, halo)] = jnp.zeros((halo, channels), ci.dtype)
+            cx[pl.ds(0, halo)] = jnp.zeros((halo, channels), cx.dtype)
+
+        @pl.when(jnp.logical_and(i == 2, sp > 0))
+        def _():
+            for k in range(2):
+                halo_copy(k, (sp, core_peer)).wait_recv()
+
+        conv(start)
 
         def some(n, c):
             cols = pl.ds(pl.multiple_of(n * tile, tile), tile)
-            got = jnp.dot(
-                mix[pl.ds(pl.multiple_of(owner * rows, rows), rows)], ow[:, cols], preferred_element_type=jnp.float32
-            )
-
-            @pl.when(i % 2 == 0)
+            got = jnp.dot(mix[pl.ds(start, piece)], ow[:, cols], preferred_element_type=jnp.float32)
+
+            @pl.when(second)
             def _():
-                part_out[i // 2, :, cols] = bf16(got)
-
-            @pl.when(i % 2 == 1)
+                acc[p, :, cols] = got
+
+            @pl.when(jnp.logical_not(second))
             def _():
-                acc[:, cols] = got
+                part_out[2 * phase + p, :, cols] = bf16(got)
 
             return c
 
         lax.fori_loop(0, depth // tile, some, 0)
 
-        @pl.when(i == 0)
-        def _():
-            core_copy(0).start()
-
-        @pl.when(i == 1)
-        def _():
-            core_copy(0).wait_recv()
+        @pl.when(jnp.logical_not(second))
+        def _():
+            core_copy(phase, p).start()
+
+        @pl.when(jnp.logical_and(second, phase == 0))
+        def _():
+            core_copy(0, p).wait_recv()
 
             def add(r, c):
                 at = pl.ds(pl.multiple_of(r * 16, 16), 16)
-                for k in range(2):
-                    src = pl.ds(pl.multiple_of(k * piece + r * 16, 16), 16)
-                    x_out[k, at] = bf16(acc[src] + f32(part_in[0, src]))
+                x_out[p, at] = bf16(acc[p, at] + f32(part_in[p, at]))
                 return c
 
             lax.fori_loop(0, piece // 16, add, 0)
-            x_copy(0).start()
-            x_copy(1).start()
-
-        @pl.when(i == 2)
-        def _():
-            core_copy(1).start()
+            x_copy(p).start()
 
         return carry
 
-    lax.fori_loop(0, 4, projected, 0)
-    core_copy(1).wait_recv()
+    lax.fori_loop(0, 8, projected, 0)
     loads[4].wait()
     loads[5].wait()
 
@@ -454,8 +471,8 @@
     def normalize(c):
         def some(r, carry):
             at = pl.ds(pl.multiple_of(r * 16, 16), 16)
-            src = pl.ds(pl.multiple_of(c * piece + r * 16, 16), 16)
-            total = acc[src] + f32(part_in[1, src]) + f32(x_in[c, at])
+            src = pl.ds(pl.multiple_of((1 - c) * piece + r * 16, 16), 16)
+            total = acc[c, at] + f32(part_in[2 + c, at]) + f32(x_in[c, at])
             mixed = jax.nn.sigmoid(f32(mg[src])) * total
             state = bf16(f32(res[src]) + rms_scale(mixed, mgain[...]))
             P[1 + c, at] = state
@@ -477,6 +494,7 @@
     relay(0, 0)
     weight_copy(0, 1).start()
     weight_copy(0, 2).start()
+    core_copy(1, 0).wait_recv()
     x_copy(0).wait_recv()
     normalize(0)
     send_own(0, False)
@@ -485,6 +503,7 @@
     def _():
         send_own(0, True)
 
+    core_copy(1, 1).wait_recv()
     x_copy(1).wait_recv()
     normalize(1)
 
@@ -495,18 +514,21 @@
     relay(1, 0)
     weight_copy(1, 1).start()
     weight_copy(1, 2).start()
-    for k in range(6, 10):
+    for k in range(6, 9):
         loads[k].wait()
     for away in range(1, 4):
         slot = (own + away) % 4
-        remote(table_hbm, T.at[pl.ds(2 * slot, 2)], tab_s.at[away], tab_r.at[slot], (sp, core_peer)).wait_recv()
+        at = T.at[pl.ds(2 * slot, 2)]
+        remote(at, at, tab_s.at[away], tab_r.at[slot], (sp, core_peer)).wait_recv()
 
     def hidden(item, k):
         gate, up = ((g1, u1), (g2, u2))[k]
         x = X[item]
         first = jnp.dot(x, gate[...], preferred_element_type=jnp.float32)
         second = jnp.dot(x, up[...], preferred_element_type=jnp.float32)
-        share = jnp.dot(T[item], picks[k], preferred_element_type=jnp.float32)
+        share = lax.dot_general(
+            T[item], picks[k], (((0,), (0,)), ((), ())), preferred_element_type=jnp.float32
+        )
         H[item, :, k * width : (k + 1) * width] = bf16(jax.nn.silu(first) * second * share)
 
     def sum_copy(item):
@@ -520,7 +542,7 @@
 
     def out_copy(c):
         return pltpu.make_async_copy(
-            S.at[2 * own + c], out_hbm.at[pl.ds(pl.multiple_of(c * piece, piece), piece)], out_sem.at[c]
+            S.at[2 * own + c], out_hbm.at[pl.ds(pl.multiple_of((1 - c) * piece, piece), piece)], out_sem.at[c]
         )
 
     def came(at):
@@ -621,7 +643,8 @@
 
     for c in range(2):
         out_copy(c).wait()
-        core_copy(c).wait_send()
+        core_copy(0, c).wait_send()
+        core_copy(1, c).wait_send()
         x_copy(c).wait_send()
 
     @pl.when(sp < count - 1)
@@ -661,9 +684,6 @@
     tokens, channels = conv_inner.shape
     width = gate_experts.shape[2]
     piece = rows // 2
-    table = routing_table(expert_ids, group_share, pair_scores, rows, count)
-    lanes = table.shape[1]
-    table = table.reshape(2, piece, lanes)
     halo = 16
     half_type, full = jnp.bfloat16, jnp.float32
     hbm = pl.BlockSpec(memory_space=pl.ANY)
@@ -672,7 +692,7 @@
     return pl.pallas_call(
         mega_kernel,
         out_shape=jax.ShapeDtypeStruct((rows, depth), half_type),
-        in_specs=[hbm, hbm, hbm, vmem, hbm, hbm, hbm, vmem, vmem, hbm, hbm, hbm, hbm],
+        in_specs=[hbm, hbm, hbm, vmem, hbm, hbm, hbm, vmem, vmem, vmem, vmem, vmem, hbm, hbm, hbm],
         out_specs=hbm,
         scratch_shapes=[
             pltpu.VMEM((halo + tokens, channels), half_type),
@@ -682,13 +702,13 @@
             pltpu.VMEM((rows, depth), half_type),
             pltpu.VMEM((rows, depth), half_type),
             pltpu.VMEM((tokens, channels), half_type),
-            pltpu.VMEM((rows, depth), full),
-            pltpu.VMEM((2, rows, depth), half_type),
-            pltpu.VMEM((2, rows, depth), half_type),
+            pltpu.VMEM((2, piece, depth), full),
+            pltpu.VMEM((4, piece, depth), half_type),
+            pltpu.VMEM((4, piece, depth), half_type),
             pltpu.VMEM((2, piece, depth), half_type),
             pltpu.VMEM((2, piece, depth), half_type),
             pltpu.VMEM((8, piece, depth), half_type),
-            pltpu.VMEM((8, piece, lanes), half_type),
+            pltpu.VMEM((8, 2 * count, piece), half_type),
             pltpu.VMEM((13, piece, depth), half_type),
             pltpu.VMEM((8, piece, depth), half_type),
             pltpu.VMEM((8, piece, 2 * width), half_type),
@@ -697,14 +717,14 @@
             pltpu.VMEM((depth, width), half_type),
             pltpu.VMEM((depth, width), half_type),
             pltpu.VMEM((2 * width, depth), half_type),
-            pltpu.VMEM((2, lanes, width), half_type),
-            dma((10,)),
+            pltpu.VMEM((2, 2 * count, width), half_type),
+            dma((9,)),
             dma((2,)),
             dma((2,)),
             dma((4,)),
             dma((4,)),
-            dma((2,)),
-            dma((2,)),
+            dma((4,)),
+            dma((4,)),
             dma((2,)),
             dma((2,)),
             dma((12,)),
@@ -721,7 +741,7 @@
         name="layer",
     )(
         conv_outer, conv_inner, conv_input, conv_taps, out_weight, mix_gate, residual,
-        mix_gain[None, :], expert_gain[None, :], table, gate_experts, up_experts, down_experts,
+        mix_gain[None, :], expert_gain[None, :], expert_ids.T, pair_scores.T, group_share[None, :], gate_experts, up_experts, down_experts,
     )
 
 

time: 120 us -> 113 us (0.942); the launches traced: 120 us -> 111 us
  Pallas kernels: 113 us -> 109 us
  other arithmetic: 3.78 us -> 0 us
    pallas_call x1, Pallas kernels: 113 us -> 109 us  [mega(): pl.pallas_call(mega_kernel, out_shape=jax.ShapeDtypeStruct((rows, depth),...]
where the time goes in v1:
time: 113 us; the launch traced here: 111 us
  Pallas kernels  109 us (96%)
  local copies, waits for them, and re-layouts  2.09 us (2%)
    pallas_call x1, Pallas kernels, mega(): pl.pallas_call(mega_kernel, out_shape=jax.ShapeDtypeStruct((rows, depth),...  109 us

profile of v1, /device:TPU:12, one launch (start us, length us, event | category | flops | bytes accessed | tf_op | source)
XLA Modules:
  0.0 111.3 jit_solution(1659275377830892052)
XLA Ops:
  0.0 109.2 %layer.1 = bf16[192,2048]{1,0:T(8,128)(2,1)} custom-call(bf16[768,512]{1,0:T(8,128)(2,1)} %co_hbm.1, bf16[768,512]{1,0:T(8,128)(2,1)} %ci_hbm.1, bf16[768,512]{1,0:T(8,128)(2,1)} %cx_hbm.1, f32[3,512]{1,0:T(4,128)} %taps.1, bf16[512,2048]{1,0:T(8,128)(2,1)} %ow_hbm.1, bf16[192,2048]{1,0:T(8,128)(2,1)} %mg_hbm.1, bf16[192,2048]{1,0:T(8,128)(2,1)} %res_hbm.1, ...), custom_call_target="tpu_custom_call" | custom-call | tf_op jit(solution)/shard_map/layer/pallas_call | solution.py:692
  109.2 2.1 %copy.17 = bf16[192,2048]{1,0:T(8,128)(2,1)} copy(bf16[192,2048]{1,0:T(8,128)(2,1)} %layer.1) | data formatting | bytes 1572864

commit v2 on v1

--- a/solution.py
+++ b/solution.py
@@ -188,19 +188,20 @@
     1 | OWN,
     2 | OWN | ARRIVE,
     4 | OWN | ARRIVE,
+    6 | OWN | ARRIVE,
     0,
-    0,
-    4 | OTHER | OUT,
-    2 | OTHER,
-    6 | OWN | OTHER | OUT | ARRIVE,
+    6 | OTHER | OUT,
+    4 | OTHER,
+    7 | OWN | OTHER | OUT | ARRIVE,
+    4 | OUT,
+    2 | OTHER | OUT,
+    5 | OWN | OTHER | OUT | ARRIVE,
+    3 | OWN | OTHER | OUT | ARRIVE,
     0 | OTHER,
-    7 | OWN | OTHER | OUT | ARRIVE,
     1 | OTHER,
-    5 | OWN | OTHER | OUT | ARRIVE,
-    2 | OUT,
-    3 | OWN | OTHER | OUT | ARRIVE,
     0 | OUT,
     1 | OUT,
+    0,
     0,
     0,
     0,
@@ -214,35 +215,38 @@
     4 | OWN | ARRIVE | FORWARD,
     1 | OWN | ARRIVE | FORWARD,
     6 | OWN | ARRIVE | FORWARD,
-    4 | OTHER,
     6 | OTHER,
     7 | OWN | OTHER | ARRIVE | FORWARD,
-    4 | OUT,
-    5 | OWN | OTHER | ARRIVE | FORWARD,
     6 | OUT,
+    5 | OWN | ARRIVE | FORWARD,
     1 | OTHER,
     0 | OTHER,
+    4 | OTHER,
     7 | OUT,
     0 | OUT,
+    5 | OTHER,
+    4 | OUT,
+    1 | OUT,
+    5 | OUT,
     2 | OTHER,
-    5 | OUT,
-    1 | OUT,
     3 | OTHER,
     2 | OUT,
     3 | OUT,
 )
 WEIGHTS_STEP = 6
 LATE_ACROSS = 4
-LATE_OUTWARD = 10
+LATE_OUTWARD = 9
+DOWN_RELAY = 15
+DOWN_STEP = 16
 
 
 def mega_kernel(
     co_hbm, ci_hbm, cx_hbm, taps, ow_hbm, mg_hbm, res_hbm, mgain, egain, ids, scores, group,
     g_hbm, u_hbm, d_hbm, out_hbm,
     ci, cx, co, ow, mg, res, mix, acc, part_out, part_in, x_out, x_in,
-    X, T, P, S, H, g1, u1, g2, u2, wd, picks,
+    X, T, P, S, H, HR, g1, u1, g2, u2, wd, wdo, picks,
     load_sem, halo_s, halo_r, tab_s, tab_r, core_s, core_r, xsw_s, xsw_r,
-    w_s, w_r, rows_s, rows_r, sum_s, sum_r, out_sem,
+    w_s, w_r, rows_s, rows_r, sum_s, sum_r, hid_s, hid_r, do_s, do_r, out_sem,
 ):
     sp = lax.axis_index("sp")
     tp = lax.axis_index("tp")
@@ -271,6 +275,27 @@
             src_ref=src, dst_ref=dst, send_sem=s, recv_sem=r, device_id=device, device_id_type=MESH_ID
         )
 
+    barrier = pltpu.get_barrier_semaphore()
+
+    def greet(device):
+        pl.semaphore_signal(barrier, inc=1, device_id=device, device_id_type=MESH_ID)
+
+    greet((sp, core_peer))
+    greet((sp, x_peer))
+    greet((y_peer, tp))
+    for away in range(1, 4):
+        greet(((sp + 2 * away) % count, tp))
+    has_next = jnp.logical_and(y == 1, sp < count - 1)
+    has_last = jnp.logical_and(y == 0, sp > 0)
+
+    @pl.when(has_next)
+    def _():
+        greet((sp + 1, tp))
+
+    @pl.when(has_last)
+    def _():
+        greet((sp - 1, tp))
+
     tokens = co.shape[0]
     loads = [
         pltpu.make_async_copy(ci_hbm, ci.at[pl.ds(halo, tokens)], load_sem.at[0]),
@@ -301,27 +326,6 @@
     for p in range(2):
         T[2 * own + p] = entries[:, (1 - p) * piece : (2 - p) * piece]
 
-    barrier = pltpu.get_barrier_semaphore()
-
-    def greet(device):
-        pl.semaphore_signal(barrier, inc=1, device_id=device, device_id_type=MESH_ID)
-
-    greet((sp, core_peer))
-    greet((sp, x_peer))
-    greet((y_peer, tp))
-    for away in range(1, 4):
-        greet(((sp + 2 * away) % count, tp))
-    has_next = jnp.logical_and(y == 1, sp < count - 1)
-    has_last = jnp.logical_and(y == 0, sp > 0)
-
-    @pl.when(has_next)
-    def _():
-        greet((sp + 1, tp))
-
-    @pl.when(has_last)
-    def _():
-        greet((sp - 1, tp))
-
     pl.semaphore_wait(barrier, 6 + jnp.where(has_next, 1, 0) + jnp.where(has_last, 1, 0))
 
     def halo_copy(k, device):
@@ -356,6 +360,24 @@
     for k in range(3):
         weight_copy(k, 0).start()
 
+    part = wide // 2
+
+    def down_copy(leg):
+        if leg < 2:
+            src = d_hbm.at[0, pl.ds(pl.multiple_of(side * wide + leg * part, part), part)]
+            dst = wdo.at[pl.ds(pl.multiple_of(side * wide + leg * part, part), part)]
+            device = (line(1), tp)
+        else:
+            near = wdo.at[pl.ds(pl.multiple_of(side * wide, wide), wide)]
+            far = wdo.at[pl.ds(pl.multiple_of(width + side * wide, wide), wide)]
+            src, dst = ((near, near), (near, far), (far, far))[leg - 2]
+            device = (y_peer, tp) if leg == 3 else (sp, core_peer)
+        return remote(src, dst, do_s.at[leg], do_r.at[leg], device)
+
+    @pl.when(outer)
+    def _():
+        down_copy(0).start()
+
     def table_copy(away):
         zz = (z + away) % 4
         same = zz // 2 == half
@@ -465,8 +487,11 @@
     loads[4].wait()
     loads[5].wait()
 
-    def rows_copy(item, device, dst, at):
-        return remote(X.at[item], X.at[dst], rows_s.at[at], rows_r.at[dst], device)
+    cut = depth // 2
+
+    def rows_copy(item, device, dst, at, k):
+        cols = pl.ds(k * cut, cut)
+        return remote(X.at[item, :, cols], X.at[dst, :, cols], rows_s.at[at, k], rows_r.at[dst, k], device)
 
     def normalize(c):
         def some(r, carry):
@@ -483,10 +508,11 @@
 
     def send_own(c, across):
         item = 2 * own + c
-        if across:
-            rows_copy(item, (line(2), tp), 4 + c, 8 + c).start()
-        else:
-            rows_copy(item, (line(1 - own), tp), item, item).start()
+        for k in range(2):
+            if across:
+                rows_copy(item, (line(2), tp), 4 + c, 8 + c, k).start()
+            else:
+                rows_copy(item, (line(1 - own), tp), item, item, k).start()
 
     def relay(k, leg):
         weight_copy(k, leg).wait_recv()
@@ -510,6 +536,7 @@
     @pl.when(outer)
     def _():
         send_own(1, False)
+        down_copy(1).start()
 
     relay(1, 0)
     weight_copy(1, 1).start()
@@ -531,22 +558,29 @@
         )
         H[item, :, k * width : (k + 1) * width] = bf16(jax.nn.silu(first) * second * share)
 
-    def sum_copy(item):
+    def sum_copy(item, m):
         slot = item // 2
         c = item % 2
         to = jnp.where(outer, 1, jnp.where(slot == 0, 0, 2))
-        dst = jnp.where(
-            outer, 1 + item, jnp.where(slot == 0, 9 + c, jnp.where(slot == 2, 11 + c, 9 + c))
+        dst = jnp.where(outer, 3 + c, jnp.where(slot == 2, 7 + c, 5 + c))
+        cols = pl.ds(pl.multiple_of(m * tile, tile), tile)
+        return remote(S.at[item, :, cols], P.at[dst, :, cols], sum_s.at[item, m], sum_r.at[dst, m], (line(to), tp))
+
+    def hidden_copy(item):
+        return remote(H.at[item], HR.at[item - 2], hid_s.at[item - 2], hid_r.at[item - 2], (line(1), tp))
+
+    def out_copy(c, m):
+        cols = pl.ds(pl.multiple_of(m * tile, tile), tile)
+        return pltpu.make_async_copy(
+            S.at[2 * own + c, :, cols],
+            out_hbm.at[pl.ds(pl.multiple_of((1 - c) * piece, piece), piece), cols],
+            out_sem.at[c, m],
         )
-        return remote(S.at[item], P.at[dst], sum_s.at[item], sum_r.at[dst], (line(to), tp))
-
-    def out_copy(c):
-        return pltpu.make_async_copy(
-            S.at[2 * own + c], out_hbm.at[pl.ds(pl.multiple_of((1 - c) * piece, piece), piece)], out_sem.at[c]
-        )
-
-    def came(at):
-        remote(S.at[0], P.at[at], sum_s.at[0], sum_r.at[at], (sp, core_peer)).wait_recv()
+
+    def came(at, m):
+        cols = pl.ds(pl.multiple_of(m * tile, tile), tile)
+        ref = P.at[at, :, cols]
+        remote(ref, ref, sum_s.at[0, m], sum_r.at[at, m], (sp, core_peer)).wait_recv()
 
     def step(n, carry):
         code = 0
@@ -560,19 +594,22 @@
         slot = item // 2
         c = item % 2
 
-        @pl.when(has(ARRIVE))
-        def _():
-            rows_copy(item, (sp, core_peer), item, item).wait_recv()
-
-        @pl.when(has(FORWARD))
-        def _():
-            across = slot == 0
-            rows_copy(
-                item,
-                (line(jnp.where(across, 2, 0)), tp),
-                jnp.where(across, 6 + c, item),
-                jnp.where(across, 10 + c, item),
-            ).start()
+        for k in range(2):
+
+            @pl.when(has(ARRIVE))
+            def _():
+                rows_copy(item, (sp, core_peer), item, item, k).wait_recv()
+
+            @pl.when(has(FORWARD))
+            def _():
+                across = slot == 0
+                rows_copy(
+                    item,
+                    (line(jnp.where(across, 2, 0)), tp),
+                    jnp.where(across, 6 + c, item),
+                    jnp.where(across, 10 + c, item),
+                    k,
+                ).start()
 
         @pl.when(jnp.logical_and(inner, n == LATE_ACROSS))
         def _():
@@ -598,6 +635,23 @@
                     at = wd.at[pl.ds(pl.multiple_of(width + (1 - side) * wide, wide), wide)]
                 remote(at, at, w_s.at[4 * k + leg], w_r.at[4 * k + leg], (sp, core_peer)).wait_recv()
 
+            @pl.when(inner)
+            def _():
+                down_copy(0).wait_recv()
+                down_copy(1).wait_recv()
+                down_copy(2).start()
+                down_copy(3).start()
+
+        @pl.when(jnp.logical_and(inner, n == DOWN_RELAY))
+        def _():
+            down_copy(3).wait_recv()
+            down_copy(4).start()
+
+        @pl.when(jnp.logical_and(inner, n == DOWN_STEP))
+        def _():
+            down_copy(2).wait_recv()
+            down_copy(4).wait_recv()
+
         @pl.when(has(OWN))
         def _():
             hidden(item, 0)
@@ -606,43 +660,61 @@
         def _():
             hidden(item, 1)
 
-        @pl.when(has(OUT))
-        def _():
-            a = jnp.where(slot == 0, 9 + c, jnp.where(outer, 0, 1 + item))
-            b = jnp.where(outer, 0, jnp.where(slot == 1, 11 + c, 0))
+        middle = jnp.logical_or(slot == 1, slot == 2)
+
+        @pl.when(jnp.logical_and(has(OUT), jnp.logical_and(outer, middle)))
+        def _():
+            hidden_copy(item).start()
+
+        @pl.when(jnp.logical_and(has(OUT), jnp.logical_not(jnp.logical_and(outer, middle))))
+        def _():
+            inner_at = jnp.where(slot == 1, 7 + c, jnp.where(slot == 2, 0, 3 + c))
+            a = jnp.where(slot == 0, 5 + c, jnp.where(outer, 0, inner_at))
             d = jnp.where(slot == own, 1 + c, 0)
 
-            @pl.when(a > 0)
+            @pl.when(middle)
             def _():
-                came(a)
-
-            @pl.when(b > 0)
-            def _():
-                came(b)
+                ref = HR.at[item - 2]
+                remote(ref, ref, hid_s.at[0], hid_r.at[item - 2], (sp, core_peer)).wait_recv()
 
             def some(m, carry):
                 cols = pl.ds(pl.multiple_of(m * tile, tile), tile)
+
+                @pl.when(a > 0)
+                def _():
+                    came(a, m)
+
                 got = jnp.dot(H[item], wd[:, cols], preferred_element_type=jnp.float32)
-                got = got + f32(P[d, :, cols]) + f32(P[a, :, cols]) + f32(P[b, :, cols])
-                S[item, :, cols] = bf16(got)
+                got = got + f32(P[d, :, cols]) + f32(P[a, :, cols])
+
+                @pl.when(middle)
+                def _():
+                    more = jnp.dot(HR[item - 2], wdo[:, cols], preferred_element_type=jnp.float32)
+                    S[item, :, cols] = bf16(got + more)
+
+                @pl.when(jnp.logical_not(middle))
+                def _():
+                    S[item, :, cols] = bf16(got)
+
+                @pl.when(slot == own)
+                def _():
+                    out_copy(c, m).start()
+
+                @pl.when(slot != own)
+                def _():
+                    sum_copy(item, m).start()
+
                 return carry
 
             lax.fori_loop(0, depth // tile, some, 0)
 
-            @pl.when(slot == own)
-            def _():
-                out_copy(c).start()
-
-            @pl.when(slot != own)
-            def _():
-                sum_copy(item).start()
-
         return carry
 
     lax.fori_loop(0, len(OUTER_STEPS), step, 0)
 
     for c in range(2):
-        out_copy(c).wait()
+        for m in range(depth // tile):
+            out_copy(c, m).wait()
         core_copy(0, c).wait_send()
         core_copy(1, c).wait_send()
         x_copy(c).wait_send()
@@ -658,21 +730,34 @@
     for away in range(1, 4):
         table_copy(away).wait_send()
 
-    def gone(item, at):
-        rows_copy(item, (sp, core_peer), item, at).wait_send()
+    def gone(at):
+        for k in range(2):
+            rows_copy(at % 8, (sp, core_peer), at % 8, at, k).wait_send()
+
+    def summed(item):
+        for m in range(depth // tile):
+            sum_copy(item, m).wait_send()
 
     for c in range(2):
-        gone(2 * own + c, 2 * own + c)
-    for i in range(3):
+        gone(2 * own + c)
+
+    @pl.when(outer)
+    def _():
         for c in range(2):
-            item = 2 * ((own + 1 + i) % 4) + c
-            remote(S.at[item], P.at[0], sum_s.at[item], sum_r.at[0], (sp, core_peer)).wait_send()
+            down_copy(c).wait_send()
+            summed(6 + c)
+            hidden_copy(2 + c).wait_send()
+            hidden_copy(4 + c).wait_send()
 
     @pl.when(inner)
     def _():
+        for leg in range(2, 5):
+            down_copy(leg).wait_send()
         for c in range(2):
             for at in (4 + c, 6 + c, 8 + c, 10 + c):
-                gone(at % 8, at)
+                gone(at)
+            for slot in (0, 2, 3):
+                summed(2 * slot + c)
 
 
 def mega(
@@ -685,6 +770,7 @@
     width = gate_experts.shape[2]
     piece = rows // 2
     halo = 16
+    tiles = depth // min(512, depth)
     half_type, full = jnp.bfloat16, jnp.float32
     hbm = pl.BlockSpec(memory_space=pl.ANY)
     vmem = pl.BlockSpec(memory_space=pltpu.VMEM)
@@ -709,13 +795,15 @@
             pltpu.VMEM((2, piece, depth), half_type),
             pltpu.VMEM((8, piece, depth), half_type),
             pltpu.VMEM((8, 2 * count, piece), half_type),
-            pltpu.VMEM((13, piece, depth), half_type),
+            pltpu.VMEM((9, piece, depth), half_type),
             pltpu.VMEM((8, piece, depth), half_type),
             pltpu.VMEM((8, piece, 2 * width), half_type),
+            pltpu.VMEM((4, piece, 2 * width), half_type),
             pltpu.VMEM((depth, width), half_type),
             pltpu.VMEM((depth, width), half_type),
             pltpu.VMEM((depth, width), half_type),
             pltpu.VMEM((depth, width), half_type),
+            pltpu.VMEM((2 * width, depth), half_type),
             pltpu.VMEM((2 * width, depth), half_type),
             pltpu.VMEM((2, 2 * count, width), half_type),
             dma((9,)),
@@ -729,11 +817,15 @@
             dma((2,)),
             dma((12,)),
             dma((12,)),
-            dma((16,)),
-            dma((8,)),
-            dma((8,)),
-            dma((13,)),
-            dma((2,)),
+            dma((16, 2)),
+            dma((8, 2)),
+            dma((8, tiles)),
+            dma((9, tiles)),
+            dma((4,)),
+            dma((4,)),
+            dma((5,)),
+            dma((5,)),
+            dma((2, tiles)),
         ],
         compiler_params=pltpu.CompilerParams(
             collective_id=0, has_side_effects=True, vmem_limit_bytes=60 * 1024 * 1024

time: 113 us -> 109 us (0.965)
  the two profiles are of different devices: /device:TPU:12 before, /device:TPU:0 now
where the time goes in v2:
time: 109 us
  Pallas kernels  107 us (98%)
  local copies, waits for them, and re-layouts  2.09 us (2%)
    pallas_call x1, Pallas kernels, mega(): pl.pallas_call(mega_kernel, out_shape=jax.ShapeDtypeStruct((rows, depth),...  107 us

profile of v2, /device:TPU:0, one launch (start us, length us, event | category | flops | bytes accessed | tf_op | source)
XLA Modules:
  0.0 108.7 jit_solution(14451286934992048199)
XLA Ops:
  0.0 106.6 %layer.1 = bf16[192,2048]{1,0:T(8,128)(2,1)} custom-call(bf16[768,512]{1,0:T(8,128)(2,1)} %co_hbm.1, bf16[768,512]{1,0:T(8,128)(2,1)} %ci_hbm.1, bf16[768,512]{1,0:T(8,128)(2,1)} %cx_hbm.1, f32[3,512]{1,0:T(4,128)} %taps.1, bf16[512,2048]{1,0:T(8,128)(2,1)} %ow_hbm.1, bf16[192,2048]{1,0:T(8,128)(2,1)} %mg_hbm.1, bf16[192,2048]{1,0:T(8,128)(2,1)} %res_hbm.1, ...), custom_call_target="tpu_custom_call" | custom-call | tf_op jit(solution)/shard_map/layer/pallas_call | solution.py:778
  106.6 2.1 %copy.17 = bf16[192,2048]{1,0:T(8,128)(2,1)} copy(bf16[192,2048]{1,0:T(8,128)(2,1)} %layer.1) | data formatting | bytes 1572864

commit v3 on v2

--- a/solution.py
+++ b/solution.py
@@ -181,63 +181,80 @@
 
 
 MESH_ID = pl.DeviceIdType.MESH
-OWN, OTHER, OUT, ARRIVE, FORWARD = 8, 16, 32, 64, 128
+OWN, OTHER, OUT, ARRIVE, FORWARD, SEND_ACROSS, SEND_OUTWARD = (8 << i for i in range(7))
+HIDDEN_READY, DOWN_READY, FAR_PASS, FAR_READY = (1024 << i for i in range(4))
+GATE_PASS, UP_PASS, DOWN_PASS = (16384 << i for i in range(3))
 
 OUTER_STEPS = (
+    1 | OWN,
     0 | OWN,
-    1 | OWN,
+    GATE_PASS,
+    6 | OWN | ARRIVE,
     2 | OWN | ARRIVE,
+    UP_PASS,
+    DOWN_PASS,
+    HIDDEN_READY,
+    6 | OTHER,
+    DOWN_READY,
+    6 | OUT,
     4 | OWN | ARRIVE,
-    6 | OWN | ARRIVE,
-    0,
-    6 | OTHER | OUT,
     4 | OTHER,
-    7 | OWN | OTHER | OUT | ARRIVE,
+    7 | OWN | ARRIVE,
+    2 | OTHER,
+    7 | OTHER,
+    7 | OUT,
     4 | OUT,
-    2 | OTHER | OUT,
-    5 | OWN | OTHER | OUT | ARRIVE,
-    3 | OWN | OTHER | OUT | ARRIVE,
+    5 | OWN | ARRIVE,
+    5 | OTHER,
+    5 | OUT,
+    3 | OWN | ARRIVE,
     0 | OTHER,
+    2 | OUT,
     1 | OTHER,
+    3 | OTHER,
     0 | OUT,
+    3 | OUT,
     1 | OUT,
-    0,
-    0,
     0,
     0,
     0,
     0,
 )
 INNER_STEPS = (
-    2 | OWN,
-    3 | OWN,
+    4 | OWN | ARRIVE | FORWARD,
     0 | OWN | ARRIVE | FORWARD,
-    4 | OWN | ARRIVE | FORWARD,
     1 | OWN | ARRIVE | FORWARD,
     6 | OWN | ARRIVE | FORWARD,
+    SEND_ACROSS,
+    2 | OWN,
+    FAR_PASS,
+    7 | OWN | ARRIVE | FORWARD,
+    GATE_PASS,
+    UP_PASS,
+    SEND_OUTWARD,
+    DOWN_PASS,
+    HIDDEN_READY,
+    0 | OTHER,
+    DOWN_READY,
+    2 | OTHER,
     6 | OTHER,
-    7 | OWN | OTHER | ARRIVE | FORWARD,
+    1 | OTHER,
     6 | OUT,
     5 | OWN | ARRIVE | FORWARD,
-    1 | OTHER,
-    0 | OTHER,
-    4 | OTHER,
+    5 | OTHER,
+    7 | OTHER,
     7 | OUT,
     0 | OUT,
-    5 | OTHER,
+    4 | OTHER,
+    FAR_READY,
     4 | OUT,
     1 | OUT,
     5 | OUT,
-    2 | OTHER,
+    3 | OWN,
+    2 | OUT,
     3 | OTHER,
-    2 | OUT,
     3 | OUT,
 )
-WEIGHTS_STEP = 6
-LATE_ACROSS = 4
-LATE_OUTWARD = 9
-DOWN_RELAY = 15
-DOWN_STEP = 16
 
 
 def mega_kernel(
@@ -283,8 +300,12 @@
     greet((sp, core_peer))
     greet((sp, x_peer))
     greet((y_peer, tp))
-    for away in range(1, 4):
-        greet(((sp + 2 * away) % count, tp))
+    greet((line(1 - own), tp))
+
+    @pl.when(inner)
+    def _():
+        greet((line(2), tp))
+
     has_next = jnp.logical_and(y == 1, sp < count - 1)
     has_last = jnp.logical_and(y == 0, sp > 0)
 
@@ -326,7 +347,7 @@
     for p in range(2):
         T[2 * own + p] = entries[:, (1 - p) * piece : (2 - p) * piece]
 
-    pl.semaphore_wait(barrier, 6 + jnp.where(has_next, 1, 0) + jnp.where(has_last, 1, 0))
+    pl.semaphore_wait(barrier, 4 + jnp.where(inner, 1, 0) + jnp.where(has_next, 1, 0) + jnp.where(has_last, 1, 0))
 
     def halo_copy(k, device):
         src = (ci_hbm, cx_hbm)[k].at[pl.ds(tokens - halo, halo)]
@@ -378,20 +399,26 @@
     def _():
         down_copy(0).start()
 
-    def table_copy(away):
-        zz = (z + away) % 4
-        same = zz // 2 == half
-        slot = jnp.where(same, own, 3 - own)
+    def table_copy(slot, across):
+        dst = 3 - slot if across else slot
+        at = slot + (4 if across else 0)
         return remote(
-            T.at[pl.ds(2 * own, 2)],
             T.at[pl.ds(2 * slot, 2)],
-            tab_s.at[away],
-            tab_r.at[slot],
-            ((sp + 2 * away) % count, tp),
+            T.at[pl.ds(2 * dst, 2)],
+            tab_s.at[at],
+            tab_r.at[dst],
+            (line(2) if across else line(1 - own), tp),
         )
 
-    for away in range(1, 4):
-        table_copy(away).start()
+    def table_came(slot):
+        at = T.at[pl.ds(2 * slot, 2)]
+        remote(at, at, tab_s.at[0], tab_r.at[slot], (sp, core_peer)).wait_recv()
+
+    table_copy(own, False).start()
+
+    @pl.when(inner)
+    def _():
+        table_copy(1, True).start()
 
     P[0] = jnp.zeros(P.shape[1:], P.dtype)
     lane = lax.broadcasted_iota(jnp.int32, (T.shape[1], width), 0)
@@ -425,8 +452,13 @@
         at = 2 * phase + p
         return remote(part_out.at[at], part_in.at[at], core_s.at[at], core_r.at[at], (sp, core_peer))
 
-    def x_copy(p):
-        return remote(x_out.at[p], x_in.at[p], xsw_s.at[p], xsw_r.at[p], (sp, x_peer))
+    some_rows = piece // 2
+
+    def x_copy(p, k):
+        at = pl.ds(k * some_rows, some_rows)
+        return remote(
+            x_out.at[p, at], x_in.at[p, at], xsw_s.at[2 * p + k], xsw_r.at[2 * p + k], (sp, x_peer)
+        )
 
     def projected(i, carry):
         phase = i // 4
@@ -478,8 +510,10 @@
                 x_out[p, at] = bf16(acc[p, at] + f32(part_in[p, at]))
                 return c
 
-            lax.fori_loop(0, piece // 16, add, 0)
-            x_copy(p).start()
+            steps = some_rows // 16
+            for k in range(2):
+                lax.fori_loop(k * steps, (k + 1) * steps, add, 0)
+                x_copy(p, k).start()
 
         return carry
 
@@ -487,13 +521,11 @@
     loads[4].wait()
     loads[5].wait()
 
-    cut = depth // 2
-
     def rows_copy(item, device, dst, at, k):
-        cols = pl.ds(k * cut, cut)
-        return remote(X.at[item, :, cols], X.at[dst, :, cols], rows_s.at[at, k], rows_r.at[dst, k], device)
-
-    def normalize(c):
+        some = pl.ds(k * some_rows, some_rows)
+        return remote(X.at[item, some], X.at[dst, some], rows_s.at[at, k], rows_r.at[dst, k], device)
+
+    def normalize(c, k):
         def some(r, carry):
             at = pl.ds(pl.multiple_of(r * 16, 16), 16)
             src = pl.ds(pl.multiple_of((1 - c) * piece + r * 16, 16), 16)
@@ -504,38 +536,55 @@
             X[2 * own + c, at] = bf16(rms_scale(f32(state), egain[...]))
             return carry
 
-        lax.fori_loop(0, piece // 16, some, 0)
-
-    def send_own(c, across):
+        steps = some_rows // 16
+        lax.fori_loop(k * steps, (k + 1) * steps, some, 0)
+
+    def send_own(c, k, across):
         item = 2 * own + c
-        for k in range(2):
-            if across:
-                rows_copy(item, (line(2), tp), 4 + c, 8 + c, k).start()
-            else:
-                rows_copy(item, (line(1 - own), tp), item, item, k).start()
+        if across:
+            rows_copy(item, (line(2), tp), 4 + c, 8 + c, k).start()
+        else:
+            rows_copy(item, (line(1 - own), tp), item, item, k).start()
 
     def relay(k, leg):
         weight_copy(k, leg).wait_recv()
+
+    @pl.when(inner)
+    def _():
+        table_came(0)
+        table_copy(0, True).start()
+        table_came(2)
+        table_copy(2, False).start()
+
+    core_copy(1, 0).wait_recv()
+    for k in range(2):
+        x_copy(0, k).wait_recv()
+        normalize(0, k)
+        send_own(0, k, False)
+
+        @pl.when(inner)
+        def _():
+            send_own(0, k, True)
+
+    @pl.when(inner)
+    def _():
+        table_came(3)
+        table_copy(3, False).start()
 
     relay(0, 0)
     weight_copy(0, 1).start()
     weight_copy(0, 2).start()
-    core_copy(1, 0).wait_recv()
-    x_copy(0).wait_recv()
-    normalize(0)
-    send_own(0, False)
-
-    @pl.when(inner)
-    def _():
-        send_own(0, True)
-
     core_copy(1, 1).wait_recv()
-    x_copy(1).wait_recv()
-    normalize(1)
+    for k in range(2):
+        x_copy(1, k).wait_recv()
+        normalize(1, k)
+
+        @pl.when(outer)
+        def _():
+            send_own(1, k, False)
 
     @pl.when(outer)
     def _():
-        send_own(1, False)
         down_copy(1).start()
 
     relay(1, 0)
@@ -543,10 +592,11 @@
     weight_copy(1, 2).start()
     for k in range(6, 9):
         loads[k].wait()
-    for away in range(1, 4):
-        slot = (own + away) % 4
-        at = T.at[pl.ds(2 * slot, 2)]
-        remote(at, at, tab_s.at[away], tab_r.at[slot], (sp, core_peer)).wait_recv()
+
+    @pl.when(outer)
+    def _():
+        for slot in range(1, 4):
+            table_came(slot)
 
     def hidden(item, k):
         gate, up = ((g1, u1), (g2, u2))[k]
@@ -611,44 +661,60 @@
                     k,
                 ).start()
 
-        @pl.when(jnp.logical_and(inner, n == LATE_ACROSS))
-        def _():
-            send_own(1, True)
-
-        @pl.when(jnp.logical_and(inner, n == LATE_OUTWARD))
-        def _():
-            send_own(1, False)
-
-        @pl.when(n == WEIGHTS_STEP)
+        @pl.when(has(SEND_ACROSS))
+        def _():
+            for k in range(2):
+                send_own(1, k, True)
+
+        @pl.when(has(SEND_OUTWARD))
+        def _():
+            for k in range(2):
+                send_own(1, k, False)
+
+        @pl.when(has(GATE_PASS))
         def _():
             relay(0, 2)
             weight_copy(0, 3).start()
+
+        @pl.when(has(UP_PASS))
+        def _():
             relay(1, 2)
             weight_copy(1, 3).start()
+
+        @pl.when(has(DOWN_PASS))
+        def _():
             relay(2, 0)
             weight_copy(2, 1).start()
-            for k, leg in ((0, 1), (1, 1), (0, 3), (1, 3), (2, 1)):
-                got = pl.multiple_of((core_peer if leg == 1 else 3 - tp) * quarter, quarter)
-                if k < 2:
-                    at = (g2, u2)[k].at[pl.ds(got, quarter)]
-                else:
-                    at = wd.at[pl.ds(pl.multiple_of(width + (1 - side) * wide, wide), wide)]
-                remote(at, at, w_s.at[4 * k + leg], w_r.at[4 * k + leg], (sp, core_peer)).wait_recv()
-
-            @pl.when(inner)
-            def _():
-                down_copy(0).wait_recv()
-                down_copy(1).wait_recv()
-                down_copy(2).start()
-                down_copy(3).start()
-
-        @pl.when(jnp.logical_and(inner, n == DOWN_RELAY))
+
+        def weight_came(k, leg):
+            got = pl.multiple_of((core_peer if leg == 1 else 3 - tp) * quarter, quarter)
+            if k < 2:
+                at = (g2, u2)[k].at[pl.ds(got, quarter)]
+            else:
+                at = wd.at[pl.ds(pl.multiple_of(width + (1 - side) * wide, wide), wide)]
+            remote(at, at, w_s.at[4 * k + leg], w_r.at[4 * k + leg], (sp, core_peer)).wait_recv()
+
+        @pl.when(has(HIDDEN_READY))
+        def _():
+            for k in range(2):
+                weight_came(k, 1)
+                weight_came(k, 3)
+
+        @pl.when(has(DOWN_READY))
+        def _():
+            weight_came(2, 1)
+
+        @pl.when(has(FAR_PASS))
+        def _():
+            down_copy(0).wait_recv()
+            down_copy(1).wait_recv()
+            down_copy(2).start()
+            down_copy(3).start()
+
+        @pl.when(has(FAR_READY))
         def _():
             down_copy(3).wait_recv()
             down_copy(4).start()
-
-        @pl.when(jnp.logical_and(inner, n == DOWN_STEP))
-        def _():
             down_copy(2).wait_recv()
             down_copy(4).wait_recv()
 
@@ -717,7 +783,8 @@
             out_copy(c, m).wait()
         core_copy(0, c).wait_send()
         core_copy(1, c).wait_send()
-        x_copy(c).wait_send()
+        x_copy(c, 0).wait_send()
+        x_copy(c, 1).wait_send()
 
     @pl.when(sp < count - 1)
     def _():
@@ -727,8 +794,15 @@
     for k in range(3):
         for leg in range(4 if k < 2 else 2):
             weight_copy(k, leg).wait_send()
-    for away in range(1, 4):
-        table_copy(away).wait_send()
+    table_copy(own, False).wait_send()
+
+    @pl.when(inner)
+    def _():
+        table_copy(1, True).wait_send()
+        table_copy(0, True).wait_send()
+        table_copy(2, False).wait_send()
+        table_copy(3, False).wait_send()
+
 
     def gone(at):
         for k in range(2):
@@ -809,12 +883,12 @@
             dma((9,)),
             dma((2,)),
             dma((2,)),
+            dma((8,)),
             dma((4,)),
             dma((4,)),
             dma((4,)),
             dma((4,)),
-            dma((2,)),
-            dma((2,)),
+            dma((4,)),
             dma((12,)),
             dma((12,)),
             dma((16, 2)),

time: 109 us -> 103 us (0.945)
  the two profiles are of different devices: /device:TPU:0 before, /device:TPU:12 now
where the time goes in v3:
time: 103 us; the launch traced here: 101 us
  Pallas kernels  99.2 us (96%)
  local copies, waits for them, and re-layouts  2.09 us (2%)
    pallas_call x1, Pallas kernels, mega(): pl.pallas_call(mega_kernel, out_shape=jax.ShapeDtypeStruct((rows, depth),...  99.2 us
    unnamed x1, local copies, waits for them, and re-layouts  2.09 us

profile of v3, /device:TPU:12, one launch (start us, length us, event | category | flops | bytes accessed | tf_op | source)
XLA Modules:
  0.0 101.3 jit_solution(13961112009025249017)
XLA Ops:
  0.0 99.2 %layer.1 = bf16[192,2048]{1,0:T(8,128)(2,1)} custom-call(bf16[768,512]{1,0:T(8,128)(2,1)} %co_hbm.1, bf16[768,512]{1,0:T(8,128)(2,1)} %ci_hbm.1, bf16[768,512]{1,0:T(8,128)(2,1)} %cx_hbm.1, f32[3,512]{1,0:T(4,128)} %taps.1, bf16[512,2048]{1,0:T(8,128)(2,1)} %ow_hbm.1, bf16[192,2048]{1,0:T(8,128)(2,1)} %mg_hbm.1, bf16[192,2048]{1,0:T(8,128)(2,1)} %res_hbm.1, ...), custom_call_target="tpu_custom_call" | custom-call | tf_op jit(solution)/shard_map/layer/pallas_call | solution.py:852
  99.2 2.1 %copy.17 = bf16[192,2048]{1,0:T(8,128)(2,1)} copy(bf16[192,2048]{1,0:T(8,128)(2,1)} %layer.1) | data formatting | bytes 1572864

commit v4 on v3

--- a/solution.py
+++ b/solution.py
@@ -182,39 +182,52 @@
 
 MESH_ID = pl.DeviceIdType.MESH
 OWN, OTHER, OUT, ARRIVE, FORWARD, SEND_ACROSS, SEND_OUTWARD = (8 << i for i in range(7))
-HIDDEN_READY, DOWN_READY, FAR_PASS, FAR_READY = (1024 << i for i in range(4))
-GATE_PASS, UP_PASS, DOWN_PASS = (16384 << i for i in range(3))
+HIDDEN_READY, DOWN_READY, FAR_PASS, FAR_READY = (8 << i for i in range(7, 11))
+GATE_PASS, UP_PASS, FIRST_PASS, DOWN_PASS = (8 << i for i in range(11, 15))
+LATE_RELAY, LATE_PASS, LATER, LATE_READY = (8 << i for i in range(15, 19))
 
 OUTER_STEPS = (
     1 | OWN,
-    0 | OWN,
+    4 | OWN | ARRIVE,
+    DOWN_PASS,
+    FIRST_PASS,
+    UP_PASS,
     GATE_PASS,
+    DOWN_READY,
+    HIDDEN_READY,
+    4 | OTHER,
+    4 | OUT,
     6 | OWN | ARRIVE,
-    2 | OWN | ARRIVE,
-    UP_PASS,
-    DOWN_PASS,
-    HIDDEN_READY,
+    LATE_RELAY,
     6 | OTHER,
-    DOWN_READY,
     6 | OUT,
-    4 | OWN | ARRIVE,
-    4 | OTHER,
     7 | OWN | ARRIVE,
-    2 | OTHER,
     7 | OTHER,
     7 | OUT,
-    4 | OUT,
+    LATE_PASS,
+    LATE_READY,
+    7 | OUT | LATER,
+    6 | OUT | LATER,
+    2 | OWN | ARRIVE,
     5 | OWN | ARRIVE,
     5 | OTHER,
     5 | OUT,
+    4 | OUT | LATER,
+    2 | OTHER,
     3 | OWN | ARRIVE,
+    3 | OTHER,
+    3 | OUT,
+    0 | OWN,
     0 | OTHER,
+    1 | OTHER,
+    1 | OUT,
     2 | OUT,
-    1 | OTHER,
-    3 | OTHER,
+    1 | OUT | LATER,
     0 | OUT,
-    3 | OUT,
-    1 | OUT,
+    0 | OUT | LATER,
+    0,
+    0,
+    0,
     0,
     0,
     0,
@@ -223,37 +236,49 @@
 INNER_STEPS = (
     4 | OWN | ARRIVE | FORWARD,
     0 | OWN | ARRIVE | FORWARD,
+    2 | OWN,
+    3 | OWN,
     1 | OWN | ARRIVE | FORWARD,
     6 | OWN | ARRIVE | FORWARD,
+    DOWN_PASS,
     SEND_ACROSS,
-    2 | OWN,
+    FIRST_PASS,
+    GATE_PASS,
+    7 | OWN | ARRIVE | FORWARD,
+    DOWN_READY,
+    UP_PASS,
     FAR_PASS,
-    7 | OWN | ARRIVE | FORWARD,
-    GATE_PASS,
-    UP_PASS,
+    HIDDEN_READY,
+    4 | OTHER,
+    LATE_RELAY,
+    6 | OTHER,
+    4 | OUT,
+    5 | OWN | ARRIVE | FORWARD,
+    7 | OTHER,
+    6 | OUT,
     SEND_OUTWARD,
-    DOWN_PASS,
-    HIDDEN_READY,
+    7 | OUT,
+    LATE_PASS,
+    5 | OTHER,
     0 | OTHER,
-    DOWN_READY,
+    LATE_READY,
+    1 | OTHER,
+    7 | OUT | LATER,
+    1 | OUT,
+    6 | OUT | LATER,
     2 | OTHER,
-    6 | OTHER,
-    1 | OTHER,
-    6 | OUT,
-    5 | OWN | ARRIVE | FORWARD,
-    5 | OTHER,
-    7 | OTHER,
-    7 | OUT,
+    1 | OUT | LATER,
+    FAR_READY,
+    5 | OUT,
     0 | OUT,
-    4 | OTHER,
-    FAR_READY,
-    4 | OUT,
-    1 | OUT,
-    5 | OUT,
-    3 | OWN,
+    3 | OTHER,
+    5 | OUT | LATER,
+    0 | OUT | LATER,
+    4 | OUT | LATER,
+    3 | OUT,
+    3 | OUT | LATER,
     2 | OUT,
-    3 | OTHER,
-    3 | OUT,
+    2 | OUT | LATER,
 )
 
 
@@ -358,28 +383,42 @@
         for k in range(2):
             halo_copy(k, (sp + 1, tp)).start()
 
-    quarter = depth // 4
+    eighth = depth // 8
     wide = width // 2
-    mine = pl.multiple_of(tp * quarter, quarter)
-    theirs = pl.multiple_of(x_peer * quarter, quarter)
     side = tp % 2
+    tile = min(512, depth)
+    tiles = depth // tile
+    quarter = width // 4
+    first = jnp.where(tp // 2 == 0, side, 6 + side)
+    lacking = jnp.where(tp // 2 == 0, 6 + side, side)
 
     def weight_copy(k, leg):
-        at = 4 * k + leg
-        if k < 2:
-            buf = (g2, u2)[k]
-            rows_at = pl.ds(theirs if leg == 3 else mine, quarter)
-            src = (g_hbm, u_hbm)[k].at[0, rows_at] if leg == 0 else buf.at[rows_at]
-            dst = buf.at[rows_at]
-        else:
-            rows_at = pl.ds(pl.multiple_of(width + side * wide, wide), wide)
-            src = d_hbm.at[0, pl.ds(pl.multiple_of(side * wide, wide), wide)] if leg == 0 else wd.at[rows_at]
-            dst = wd.at[rows_at]
+        block = (first, 2 + side, 4 + side, first, 2 + side, 4 + side, lacking, first)[leg]
+        at = pl.ds(pl.multiple_of(block * eighth, eighth), eighth)
+        buf = (g2, u2)[k]
+        src = (g_hbm, u_hbm)[k].at[0, at] if leg < 3 else buf.at[at]
+        device = (y_peer, tp) if leg < 3 else (sp, core_peer) if leg < 7 else (sp, x_peer)
+        return remote(src, buf.at[at], w_s.at[8 * k + leg], w_r.at[8 * k + leg], device)
+
+    def tile_copy(t, leg):
+        row = (x_peer if leg == 3 else tp) * quarter
+        cols = pl.ds(t * tile, tile)
+        dst = wd.at[pl.ds(pl.multiple_of(width + row, quarter), quarter), cols]
+        src = d_hbm.at[0, pl.ds(pl.multiple_of(row, quarter), quarter), cols] if leg == 0 else dst
         device = ((y_peer, tp), (sp, core_peer), (sp, x_peer), (sp, core_peer))[leg]
-        return remote(src, dst, w_s.at[at], w_r.at[at], device)
-
-    for k in range(3):
+        return remote(src, dst, w_s.at[16 + 4 * t + leg], w_r.at[16 + 4 * t + leg], device)
+
+    early = range(tiles // 2)
+    late = range(tiles // 2, tiles)
+    for k in range(2):
         weight_copy(k, 0).start()
+    for t in early:
+        tile_copy(t, 0).start()
+    for k in range(2):
+        weight_copy(k, 1).start()
+        weight_copy(k, 2).start()
+    for t in late:
+        tile_copy(t, 0).start()
 
     part = wide // 2
 
@@ -445,7 +484,6 @@
 
         lax.fori_loop(0, piece // run, some, 0)
 
-    tile = min(512, depth)
     loads[3].wait()
 
     def core_copy(phase, p):
@@ -546,8 +584,15 @@
         else:
             rows_copy(item, (line(1 - own), tp), item, item, k).start()
 
-    def relay(k, leg):
-        weight_copy(k, leg).wait_recv()
+    def weight_on(k, came, *legs):
+        weight_copy(k, came).wait_recv()
+        for leg in legs:
+            weight_copy(k, leg).start()
+
+    def tile_on(t, came, *legs):
+        tile_copy(t, came).wait_recv()
+        for leg in legs:
+            tile_copy(t, leg).start()
 
     @pl.when(inner)
     def _():
@@ -556,6 +601,7 @@
         table_came(2)
         table_copy(2, False).start()
 
+    weight_on(0, 0, 3, 7)
     core_copy(1, 0).wait_recv()
     for k in range(2):
         x_copy(0, k).wait_recv()
@@ -571,9 +617,7 @@
         table_came(3)
         table_copy(3, False).start()
 
-    relay(0, 0)
-    weight_copy(0, 1).start()
-    weight_copy(0, 2).start()
+    weight_on(1, 0, 3, 7)
     core_copy(1, 1).wait_recv()
     for k in range(2):
         x_copy(1, k).wait_recv()
@@ -587,9 +631,8 @@
     def _():
         down_copy(1).start()
 
-    relay(1, 0)
-    weight_copy(1, 1).start()
-    weight_copy(1, 2).start()
+    for t in early:
+        tile_on(t, 0, 1, 2)
     for k in range(6, 9):
         loads[k].wait()
 
@@ -612,12 +655,16 @@
         slot = item // 2
         c = item % 2
         to = jnp.where(outer, 1, jnp.where(slot == 0, 0, 2))
-        dst = jnp.where(outer, 3 + c, jnp.where(slot == 2, 7 + c, 5 + c))
+        dst = jnp.where(outer, jnp.where(slot == 2, 9 + c, 3 + c), jnp.where(slot == 2, 7 + c, 5 + c))
         cols = pl.ds(pl.multiple_of(m * tile, tile), tile)
         return remote(S.at[item, :, cols], P.at[dst, :, cols], sum_s.at[item, m], sum_r.at[dst, m], (line(to), tp))
 
+    def held(item):
+        return jnp.where(item == 5, 2, item - 2)
+
     def hidden_copy(item):
-        return remote(H.at[item], HR.at[item - 2], hid_s.at[item - 2], hid_r.at[item - 2], (line(1), tp))
+        at = held(item)
+        return remote(H.at[item], HR.at[at], hid_s.at[at], hid_r.at[at], (line(1), tp))
 
     def out_copy(c, m):
         cols = pl.ds(pl.multiple_of(m * tile, tile), tile)
@@ -671,38 +718,46 @@
             for k in range(2):
                 send_own(1, k, False)
 
-        @pl.when(has(GATE_PASS))
-        def _():
-            relay(0, 2)
-            weight_copy(0, 3).start()
-
-        @pl.when(has(UP_PASS))
-        def _():
-            relay(1, 2)
-            weight_copy(1, 3).start()
+        for k in range(2):
+
+            @pl.when(has((GATE_PASS, UP_PASS)[k]))
+            def _():
+                weight_on(k, 1, 4)
+                weight_on(k, 2, 5)
+
+        @pl.when(has(FIRST_PASS))
+        def _():
+            weight_on(0, 7, 6)
+            weight_on(1, 7, 6)
 
         @pl.when(has(DOWN_PASS))
         def _():
-            relay(2, 0)
-            weight_copy(2, 1).start()
-
-        def weight_came(k, leg):
-            got = pl.multiple_of((core_peer if leg == 1 else 3 - tp) * quarter, quarter)
-            if k < 2:
-                at = (g2, u2)[k].at[pl.ds(got, quarter)]
-            else:
-                at = wd.at[pl.ds(pl.multiple_of(width + (1 - side) * wide, wide), wide)]
-            remote(at, at, w_s.at[4 * k + leg], w_r.at[4 * k + leg], (sp, core_peer)).wait_recv()
+            for t in early:
+                tile_on(t, 2, 3)
+
+        @pl.when(has(LATE_RELAY))
+        def _():
+            for t in late:
+                tile_on(t, 0, 1, 2)
+
+        @pl.when(has(LATE_PASS))
+        def _():
+            for t in late:
+                tile_on(t, 2, 3)
 
         @pl.when(has(HIDDEN_READY))
         def _():
             for k in range(2):
-                weight_came(k, 1)
-                weight_came(k, 3)
-
-        @pl.when(has(DOWN_READY))
-        def _():
-            weight_came(2, 1)
+                for leg in range(3, 7):
+                    weight_copy(k, leg).wait_recv()
+
+        for flag, some_tiles in ((DOWN_READY, early), (LATE_READY, late)):
+
+            @pl.when(has(flag))
+            def _():
+                for t in some_tiles:
+                    tile_copy(t, 1).wait_recv()
+                    tile_copy(t, 3).wait_recv()
 
         @pl.when(has(FAR_PASS))
         def _():
@@ -726,7 +781,8 @@
         def _():
             hidden(item, 1)
 
-        middle = jnp.logical_or(slot == 1, slot == 2)
+        middle = jnp.logical_or(slot == 1, item == 5)
+        begins = code // LATER % 2 == 0
 
         @pl.when(jnp.logical_and(has(OUT), jnp.logical_and(outer, middle)))
         def _():
@@ -734,14 +790,14 @@
 
         @pl.when(jnp.logical_and(has(OUT), jnp.logical_not(jnp.logical_and(outer, middle))))
         def _():
-            inner_at = jnp.where(slot == 1, 7 + c, jnp.where(slot == 2, 0, 3 + c))
+            inner_at = jnp.where(slot == 1, 7 + c, jnp.where(slot == 2, jnp.where(c == 0, 9, 0), 3 + c))
             a = jnp.where(slot == 0, 5 + c, jnp.where(outer, 0, inner_at))
             d = jnp.where(slot == own, 1 + c, 0)
 
-            @pl.when(middle)
+            @pl.when(jnp.logical_and(middle, begins))
             def _():
-                ref = HR.at[item - 2]
-                remote(ref, ref, hid_s.at[0], hid_r.at[item - 2], (sp, core_peer)).wait_recv()
+                ref = HR.at[held(item)]
+                remote(ref, ref, hid_s.at[0], hid_r.at[held(item)], (sp, core_peer)).wait_recv()
 
             def some(m, carry):
                 cols = pl.ds(pl.multiple_of(m * tile, tile), tile)
@@ -755,7 +811,7 @@
 
                 @pl.when(middle)
                 def _():
-                    more = jnp.dot(HR[item - 2], wdo[:, cols], preferred_element_type=jnp.float32)
+                    more = jnp.dot(HR[held(item)], wdo[:, cols], preferred_element_type=jnp.float32)
                     S[item, :, cols] = bf16(got + more)
 
                 @pl.when(jnp.logical_not(middle))
@@ -772,7 +828,8 @@
 
                 return carry
 
-            lax.fori_loop(0, depth // tile, some, 0)
+            begin = jnp.where(begins, 0, tiles // 2)
+            lax.fori_loop(begin, begin + tiles // 2, some, 0)
 
         return carry
 
@@ -791,9 +848,12 @@
         for k in range(2):
             halo_copy(k, (sp + 1, tp)).wait_send()
 
-    for k in range(3):
-        for leg in range(4 if k < 2 else 2):
+    for k in range(2):
+        for leg in range(8):
             weight_copy(k, leg).wait_send()
+    for t in range(tiles):
+        for leg in range(4):
+            tile_copy(t, leg).wait_send()
     table_copy(own, False).wait_send()
 
     @pl.when(inner)
@@ -817,11 +877,12 @@
 
     @pl.when(outer)
     def _():
+        summed(4)
+        hidden_copy(5).wait_send()
         for c in range(2):
             down_copy(c).wait_send()
             summed(6 + c)
             hidden_copy(2 + c).wait_send()
-            hidden_copy(4 + c).wait_send()
 
     @pl.when(inner)
     def _():
@@ -869,10 +930,10 @@
             pltpu.VMEM((2, piece, depth), half_type),
             pltpu.VMEM((8, piece, depth), half_type),
             pltpu.VMEM((8, 2 * count, piece), half_type),
-            pltpu.VMEM((9, piece, depth), half_type),
+            pltpu.VMEM((11, piece, depth), half_type),
             pltpu.VMEM((8, piece, depth), half_type),
             pltpu.VMEM((8, piece, 2 * width), half_type),
-            pltpu.VMEM((4, piece, 2 * width), half_type),
+            pltpu.VMEM((3, piece, 2 * width), half_type),
             pltpu.VMEM((depth, width), half_type),
             pltpu.VMEM((depth, width), half_type),
             pltpu.VMEM((depth, width), half_type),
@@ -889,14 +950,14 @@
             dma((4,)),
             dma((4,)),
             dma((4,)),
-            dma((12,)),
-            dma((12,)),
+            dma((16 + 4 * tiles,)),
+            dma((16 + 4 * tiles,)),
             dma((16, 2)),
             dma((8, 2)),
             dma((8, tiles)),
-            dma((9, tiles)),
-            dma((4,)),
-            dma((4,)),
+            dma((11, tiles)),
+            dma((3,)),
+            dma((3,)),
             dma((5,)),
             dma((5,)),
             dma((2, tiles)),

time: 103 us -> 99.6 us (0.967)
  Pallas kernels: 99.2 us -> 95.6 us
    pallas_call x1, Pallas kernels: 99.2 us -> 95.6 us  [mega(): pl.pallas_call(mega_kernel, out_shape=jax.ShapeDtypeStruct((rows, depth),...]
where the time goes in v4:
time: 99.6 us; the launch traced here: 97.7 us
  Pallas kernels  95.6 us (96%)
  local copies, waits for them, and re-layouts  2.09 us (2%)
    pallas_call x1, Pallas kernels, mega(): pl.pallas_call(mega_kernel, out_shape=jax.ShapeDtypeStruct((rows, depth),...  95.6 us
    unnamed x1, local copies, waits for them, and re-layouts  2.09 us

profile of v4, /device:TPU:12, one launch (start us, length us, event | category | flops | bytes accessed | tf_op | source)
XLA Modules:
  0.0 97.7 jit_solution(8717708706859448618)
XLA Ops:
  0.0 95.6 %layer.1 = bf16[192,2048]{1,0:T(8,128)(2,1)} custom-call(bf16[768,512]{1,0:T(8,128)(2,1)} %co_hbm.1, bf16[768,512]{1,0:T(8,128)(2,1)} %ci_hbm.1, bf16[768,512]{1,0:T(8,128)(2,1)} %cx_hbm.1, f32[3,512]{1,0:T(4,128)} %taps.1, bf16[512,2048]{1,0:T(8,128)(2,1)} %ow_hbm.1, bf16[192,2048]{1,0:T(8,128)(2,1)} %mg_hbm.1, bf16[192,2048]{1,0:T(8,128)(2,1)} %res_hbm.1, ...), custom_call_target="tpu_custom_call" | custom-call | tf_op jit(solution)/shard_map/layer/pallas_call | solution.py:913
  95.6 2.1 %copy.17 = bf16[192,2048]{1,0:T(8,128)(2,1)} copy(bf16[192,2048]{1,0:T(8,128)(2,1)} %layer.1) | data formatting | bytes 1572864

commit v5 on v4

--- a/solution.py
+++ b/solution.py
@@ -181,50 +181,38 @@
 
 
 MESH_ID = pl.DeviceIdType.MESH
-OWN, OTHER, OUT, ARRIVE, FORWARD, SEND_ACROSS, SEND_OUTWARD = (8 << i for i in range(7))
-HIDDEN_READY, DOWN_READY, FAR_PASS, FAR_READY = (8 << i for i in range(7, 11))
-GATE_PASS, UP_PASS, FIRST_PASS, DOWN_PASS = (8 << i for i in range(11, 15))
-LATE_RELAY, LATE_PASS, LATER, LATE_READY = (8 << i for i in range(15, 19))
+OWN, OTHER, OUT, ARRIVE, FORWARD, LATER = (8 << i for i in range(6))
+SPECIAL = 8 << 6
+(DOWN_PASS, SEND_ACROSS, FIRST_PASS, GATE_PASS, UP_PASS, DOWN_READY, FAR_PASS, HIDDEN_READY, SEND_OUTWARD, LATE_RELAY, LATE_PASS, LATE_READY, FAR_READY,) = (SPECIAL << i for i in range(13))
 
 OUTER_STEPS = (
     1 | OWN,
     4 | OWN | ARRIVE,
-    DOWN_PASS,
-    FIRST_PASS,
-    UP_PASS,
-    GATE_PASS,
-    DOWN_READY,
-    HIDDEN_READY,
-    4 | OTHER,
-    4 | OUT,
+    0 | DOWN_PASS | FIRST_PASS | UP_PASS,
+    4 | OTHER | OUT | GATE_PASS | DOWN_READY | HIDDEN_READY,
     6 | OWN | ARRIVE,
-    LATE_RELAY,
-    6 | OTHER,
-    6 | OUT,
-    7 | OWN | ARRIVE,
-    7 | OTHER,
-    7 | OUT,
-    LATE_PASS,
-    LATE_READY,
-    7 | OUT | LATER,
+    6 | OTHER | OUT | LATE_RELAY,
+    7 | OWN | OTHER | OUT | ARRIVE,
+    7 | OUT | LATER | LATE_PASS | LATE_READY,
     6 | OUT | LATER,
     2 | OWN | ARRIVE,
-    5 | OWN | ARRIVE,
-    5 | OTHER,
-    5 | OUT,
+    5 | OWN | OTHER | OUT | ARRIVE,
     4 | OUT | LATER,
     2 | OTHER,
-    3 | OWN | ARRIVE,
-    3 | OTHER,
-    3 | OUT,
-    0 | OWN,
-    0 | OTHER,
-    1 | OTHER,
-    1 | OUT,
+    3 | OWN | OTHER | OUT | ARRIVE,
+    0 | OWN | OTHER,
+    1 | OTHER | OUT,
     2 | OUT,
     1 | OUT | LATER,
     0 | OUT,
     0 | OUT | LATER,
+    0,
+    0,
+    0,
+    0,
+    0,
+    0,
+    0,
     0,
     0,
     0,
@@ -240,36 +228,25 @@
     3 | OWN,
     1 | OWN | ARRIVE | FORWARD,
     6 | OWN | ARRIVE | FORWARD,
-    DOWN_PASS,
-    SEND_ACROSS,
-    FIRST_PASS,
-    GATE_PASS,
+    0 | DOWN_PASS | SEND_ACROSS | FIRST_PASS | GATE_PASS,
     7 | OWN | ARRIVE | FORWARD,
-    DOWN_READY,
-    UP_PASS,
-    FAR_PASS,
-    HIDDEN_READY,
-    4 | OTHER,
-    LATE_RELAY,
-    6 | OTHER,
+    0 | DOWN_READY,
+    4 | OTHER | UP_PASS | FAR_PASS | HIDDEN_READY,
+    6 | OTHER | LATE_RELAY,
     4 | OUT,
     5 | OWN | ARRIVE | FORWARD,
     7 | OTHER,
     6 | OUT,
-    SEND_OUTWARD,
-    7 | OUT,
-    LATE_PASS,
-    5 | OTHER,
+    7 | OUT | SEND_OUTWARD,
+    5 | OTHER | LATE_PASS,
     0 | OTHER,
-    LATE_READY,
-    1 | OTHER,
+    1 | OTHER | LATE_READY,
     7 | OUT | LATER,
     1 | OUT,
     6 | OUT | LATER,
     2 | OTHER,
     1 | OUT | LATER,
-    FAR_READY,
-    5 | OUT,
+    5 | OUT | FAR_READY,
     0 | OUT,
     3 | OTHER,
     5 | OUT | LATER,
@@ -691,87 +668,94 @@
         slot = item // 2
         c = item % 2
 
-        for k in range(2):
-
-            @pl.when(has(ARRIVE))
-            def _():
+        @pl.when(has(ARRIVE))
+        def _():
+            forwards = has(FORWARD)
+            across = slot == 0
+            for k in range(2):
                 rows_copy(item, (sp, core_peer), item, item, k).wait_recv()
 
-            @pl.when(has(FORWARD))
-            def _():
-                across = slot == 0
-                rows_copy(
-                    item,
-                    (line(jnp.where(across, 2, 0)), tp),
-                    jnp.where(across, 6 + c, item),
-                    jnp.where(across, 10 + c, item),
-                    k,
-                ).start()
-
-        @pl.when(has(SEND_ACROSS))
-        def _():
+                @pl.when(forwards)
+                def _():
+                    rows_copy(
+                        item,
+                        (line(jnp.where(across, 2, 0)), tp),
+                        jnp.where(across, 6 + c, item),
+                        jnp.where(across, 10 + c, item),
+                        k,
+                    ).start()
+
+        def specials():
+            @pl.when(has(DOWN_PASS))
+            def _():
+                for t in early:
+                    tile_on(t, 2, 3)
+
+            @pl.when(has(SEND_ACROSS))
+            def _():
+                for k in range(2):
+                    send_own(1, k, True)
+
+            @pl.when(has(FIRST_PASS))
+            def _():
+                weight_on(0, 7, 6)
+                weight_on(1, 7, 6)
+
             for k in range(2):
-                send_own(1, k, True)
-
-        @pl.when(has(SEND_OUTWARD))
-        def _():
-            for k in range(2):
-                send_own(1, k, False)
-
-        for k in range(2):
-
-            @pl.when(has((GATE_PASS, UP_PASS)[k]))
-            def _():
-                weight_on(k, 1, 4)
-                weight_on(k, 2, 5)
-
-        @pl.when(has(FIRST_PASS))
-        def _():
-            weight_on(0, 7, 6)
-            weight_on(1, 7, 6)
-
-        @pl.when(has(DOWN_PASS))
-        def _():
-            for t in early:
-                tile_on(t, 2, 3)
-
-        @pl.when(has(LATE_RELAY))
-        def _():
-            for t in late:
-                tile_on(t, 0, 1, 2)
-
-        @pl.when(has(LATE_PASS))
-        def _():
-            for t in late:
-                tile_on(t, 2, 3)
-
-        @pl.when(has(HIDDEN_READY))
-        def _():
-            for k in range(2):
-                for leg in range(3, 7):
-                    weight_copy(k, leg).wait_recv()
-
-        for flag, some_tiles in ((DOWN_READY, early), (LATE_READY, late)):
-
-            @pl.when(has(flag))
-            def _():
-                for t in some_tiles:
+
+                @pl.when(has((GATE_PASS, UP_PASS)[k]))
+                def _():
+                    weight_on(k, 1, 4)
+                    weight_on(k, 2, 5)
+
+            @pl.when(has(DOWN_READY))
+            def _():
+                for t in early:
                     tile_copy(t, 1).wait_recv()
                     tile_copy(t, 3).wait_recv()
 
-        @pl.when(has(FAR_PASS))
-        def _():
-            down_copy(0).wait_recv()
-            down_copy(1).wait_recv()
-            down_copy(2).start()
-            down_copy(3).start()
-
-        @pl.when(has(FAR_READY))
-        def _():
-            down_copy(3).wait_recv()
-            down_copy(4).start()
-            down_copy(2).wait_recv()
-            down_copy(4).wait_recv()
+            @pl.when(has(FAR_PASS))
+            def _():
+                down_copy(0).wait_recv()
+                down_copy(1).wait_recv()
+                down_copy(2).start()
+                down_copy(3).start()
+
+            @pl.when(has(HIDDEN_READY))
+            def _():
+                for k in range(2):
+                    for leg in range(3, 7):
+                        weight_copy(k, leg).wait_recv()
+
+            @pl.when(has(SEND_OUTWARD))
+            def _():
+                for k in range(2):
+                    send_own(1, k, False)
+
+            @pl.when(has(LATE_RELAY))
+            def _():
+                for t in late:
+                    tile_on(t, 0, 1, 2)
+
+            @pl.when(has(LATE_PASS))
+            def _():
+                for t in late:
+                    tile_on(t, 2, 3)
+
+            @pl.when(has(LATE_READY))
+            def _():
+                for t in late:
+                    tile_copy(t, 1).wait_recv()
+                    tile_copy(t, 3).wait_recv()
+
+            @pl.when(has(FAR_READY))
+            def _():
+                down_copy(3).wait_recv()
+                down_copy(4).start()
+                down_copy(2).wait_recv()
+                down_copy(4).wait_recv()
+
+        pl.when(code >= SPECIAL)(specials)
 
         @pl.when(has(OWN))
         def _():
@@ -784,11 +768,13 @@
         middle = jnp.logical_or(slot == 1, item == 5)
         begins = code // LATER % 2 == 0
 
-        @pl.when(jnp.logical_and(has(OUT), jnp.logical_and(outer, middle)))
+        short = jnp.logical_and(outer, middle)
+
+        @pl.when(jnp.logical_and(has(OUT), short))
         def _():
             hidden_copy(item).start()
 
-        @pl.when(jnp.logical_and(has(OUT), jnp.logical_not(jnp.logical_and(outer, middle))))
+        @pl.when(jnp.logical_and(has(OUT), jnp.logical_not(short)))
         def _():
             inner_at = jnp.where(slot == 1, 7 + c, jnp.where(slot == 2, jnp.where(c == 0, 9, 0), 3 + c))
             a = jnp.where(slot == 0, 5 + c, jnp.where(outer, 0, inner_at))

time: 99.6 us -> 97.9 us (0.983)
  no operation moved by 1% of the time
where the time goes in v5:
time: 97.9 us; the launch traced here: 96.8 us
  Pallas kernels  94.7 us (97%)
  local copies, waits for them, and re-layouts  2.09 us (2%)
    pallas_call x1, Pallas kernels, mega(): pl.pallas_call(mega_kernel, out_shape=jax.ShapeDtypeStruct((rows, depth),...  94.7 us
    unnamed x1, local copies, waits for them, and re-layouts  2.09 us

profile of v5, /device:TPU:12, one launch (start us, length us, event | category | flops | bytes accessed | tf_op | source)
XLA Modules:
  0.0 96.8 jit_solution(5058946178602576051)
XLA Ops:
  0.0 94.7 %layer.1 = bf16[192,2048]{1,0:T(8,128)(2,1)} custom-call(bf16[768,512]{1,0:T(8,128)(2,1)} %co_hbm.1, bf16[768,512]{1,0:T(8,128)(2,1)} %ci_hbm.1, bf16[768,512]{1,0:T(8,128)(2,1)} %cx_hbm.1, f32[3,512]{1,0:T(4,128)} %taps.1, bf16[512,2048]{1,0:T(8,128)(2,1)} %ow_hbm.1, bf16[192,2048]{1,0:T(8,128)(2,1)} %mg_hbm.1, bf16[192,2048]{1,0:T(8,128)(2,1)} %res_hbm.1, ...), custom_call_target="tpu_custom_call" | custom-call | tf_op jit(solution)/shard_map/layer/pallas_call | solution.py:899
  94.7 2.1 %copy.17 = bf16[192,2048]{1,0:T(8,128)(2,1)} copy(bf16[192,2048]{1,0:T(8,128)(2,1)} %layer.1) | data formatting | bytes 1572864

commit v6 on v5

--- a/solution.py
+++ b/solution.py
@@ -186,28 +186,29 @@
 (DOWN_PASS, SEND_ACROSS, FIRST_PASS, GATE_PASS, UP_PASS, DOWN_READY, FAR_PASS, HIDDEN_READY, SEND_OUTWARD, LATE_RELAY, LATE_PASS, LATE_READY, FAR_READY,) = (SPECIAL << i for i in range(13))
 
 OUTER_STEPS = (
+    0 | FIRST_PASS,
+    4 | OWN | ARRIVE,
+    0 | OWN,
+    0 | GATE_PASS | UP_PASS,
+    4 | OTHER | OUT | DOWN_PASS | DOWN_READY | HIDDEN_READY,
+    6 | OWN | OTHER | ARRIVE,
+    6 | OUT | LATE_RELAY,
+    7 | OWN | OTHER | OUT | ARRIVE,
+    2 | OWN | ARRIVE,
+    7 | OUT | LATER | LATE_PASS | LATE_READY,
     1 | OWN,
-    4 | OWN | ARRIVE,
-    0 | DOWN_PASS | FIRST_PASS | UP_PASS,
-    4 | OTHER | OUT | GATE_PASS | DOWN_READY | HIDDEN_READY,
-    6 | OWN | ARRIVE,
-    6 | OTHER | OUT | LATE_RELAY,
-    7 | OWN | OTHER | OUT | ARRIVE,
-    7 | OUT | LATER | LATE_PASS | LATE_READY,
+    2 | OTHER,
     6 | OUT | LATER,
-    2 | OWN | ARRIVE,
+    0 | OTHER,
+    4 | OUT | LATER,
     5 | OWN | OTHER | OUT | ARRIVE,
-    4 | OUT | LATER,
-    2 | OTHER,
-    3 | OWN | OTHER | OUT | ARRIVE,
-    0 | OWN | OTHER,
     1 | OTHER | OUT,
+    3 | OWN | ARRIVE,
     2 | OUT,
+    0 | OUT,
+    3 | OTHER | OUT,
     1 | OUT | LATER,
-    0 | OUT,
     0 | OUT | LATER,
-    0,
-    0,
     0,
     0,
     0,
@@ -224,38 +225,39 @@
 INNER_STEPS = (
     4 | OWN | ARRIVE | FORWARD,
     0 | OWN | ARRIVE | FORWARD,
-    2 | OWN,
-    3 | OWN,
     1 | OWN | ARRIVE | FORWARD,
     6 | OWN | ARRIVE | FORWARD,
-    0 | DOWN_PASS | SEND_ACROSS | FIRST_PASS | GATE_PASS,
+    0 | SEND_ACROSS | FIRST_PASS,
+    0 | DOWN_PASS | GATE_PASS,
     7 | OWN | ARRIVE | FORWARD,
-    0 | DOWN_READY,
-    4 | OTHER | UP_PASS | FAR_PASS | HIDDEN_READY,
-    6 | OTHER | LATE_RELAY,
+    3 | OWN | UP_PASS,
+    0 | FAR_PASS | SEND_OUTWARD | LATE_RELAY,
+    4 | OTHER | HIDDEN_READY,
+    7 | OTHER | DOWN_READY,
+    6 | OTHER,
     4 | OUT,
+    0 | OTHER,
     5 | OWN | ARRIVE | FORWARD,
-    7 | OTHER,
     6 | OUT,
-    7 | OUT | SEND_OUTWARD,
-    5 | OTHER | LATE_PASS,
-    0 | OTHER,
-    1 | OTHER | LATE_READY,
-    7 | OUT | LATER,
+    1 | OTHER | LATE_PASS,
+    7 | OUT,
+    5 | OTHER,
+    2 | OWN,
+    7 | OUT | LATER | LATE_READY,
     1 | OUT,
+    0 | OUT,
     6 | OUT | LATER,
     2 | OTHER,
+    3 | OTHER,
+    4 | OUT | LATER,
     1 | OUT | LATER,
+    0 | OUT | LATER,
     5 | OUT | FAR_READY,
-    0 | OUT,
-    3 | OTHER,
     5 | OUT | LATER,
-    0 | OUT | LATER,
-    4 | OUT | LATER,
+    2 | OUT,
+    2 | OUT | LATER,
     3 | OUT,
     3 | OUT | LATER,
-    2 | OUT,
-    2 | OUT | LATER,
 )
 
 
@@ -263,7 +265,7 @@
     co_hbm, ci_hbm, cx_hbm, taps, ow_hbm, mg_hbm, res_hbm, mgain, egain, ids, scores, group,
     g_hbm, u_hbm, d_hbm, out_hbm,
     ci, cx, co, ow, mg, res, mix, acc, part_out, part_in, x_out, x_in,
-    X, T, P, S, H, HR, g1, u1, g2, u2, wd, wdo, picks,
+    X, T, P, S, H, HR, stage, g1, u1, g2, u2, wd, wdo, picks,
     load_sem, halo_s, halo_r, tab_s, tab_r, core_s, core_r, xsw_s, xsw_r,
     w_s, w_r, rows_s, rows_r, sum_s, sum_r, hid_s, hid_r, do_s, do_r, out_sem,
 ):
@@ -788,21 +790,17 @@
             def some(m, carry):
                 cols = pl.ds(pl.multiple_of(m * tile, tile), tile)
 
+                stage[...] = jnp.dot(H[item], wd[:, cols], preferred_element_type=jnp.float32)
+
+                @pl.when(middle)
+                def _():
+                    stage[...] += jnp.dot(HR[held(item)], wdo[:, cols], preferred_element_type=jnp.float32)
+
                 @pl.when(a > 0)
                 def _():
                     came(a, m)
 
-                got = jnp.dot(H[item], wd[:, cols], preferred_element_type=jnp.float32)
-                got = got + f32(P[d, :, cols]) + f32(P[a, :, cols])
-
-                @pl.when(middle)
-                def _():
-                    more = jnp.dot(HR[held(item)], wdo[:, cols], preferred_element_type=jnp.float32)
-                    S[item, :, cols] = bf16(got + more)
-
-                @pl.when(jnp.logical_not(middle))
-                def _():
-                    S[item, :, cols] = bf16(got)
+                S[item, :, cols] = bf16(stage[...] + f32(P[d, :, cols]) + f32(P[a, :, cols]))
 
                 @pl.when(slot == own)
                 def _():
@@ -920,6 +918,7 @@
             pltpu.VMEM((8, piece, depth), half_type),
             pltpu.VMEM((8, piece, 2 * width), half_type),
             pltpu.VMEM((3, piece, 2 * width), half_type),
+            pltpu.VMEM((piece, min(512, depth)), full),
             pltpu.VMEM((depth, width), half_type),
             pltpu.VMEM((depth, width), half_type),
             pltpu.VMEM((depth, width), half_type),

time: 97.9 us -> 96.8 us (0.989)
  no operation moved by 1% of the time
where the time goes in v6:
time: 96.8 us; the launch traced here: 96.2 us
  Pallas kernels  94.1 us (97%)
  local copies, waits for them, and re-layouts  2.09 us (2%)
    pallas_call x1, Pallas kernels, mega(): pl.pallas_call(mega_kernel, out_shape=jax.ShapeDtypeStruct((rows, depth),...  94.1 us
    unnamed x1, local copies, waits for them, and re-layouts  2.09 us

profile of v6, /device:TPU:12, one launch (start us, length us, event | category | flops | bytes accessed | tf_op | source)
XLA Modules:
  0.0 96.2 jit_solution(2029947687636749684)
XLA Ops:
  0.0 94.1 %layer.1 = bf16[192,2048]{1,0:T(8,128)(2,1)} custom-call(bf16[768,512]{1,0:T(8,128)(2,1)} %co_hbm.1, bf16[768,512]{1,0:T(8,128)(2,1)} %ci_hbm.1, bf16[768,512]{1,0:T(8,128)(2,1)} %cx_hbm.1, f32[3,512]{1,0:T(4,128)} %taps.1, bf16[512,2048]{1,0:T(8,128)(2,1)} %ow_hbm.1, bf16[192,2048]{1,0:T(8,128)(2,1)} %mg_hbm.1, bf16[192,2048]{1,0:T(8,128)(2,1)} %res_hbm.1, ...), custom_call_target="tpu_custom_call" | custom-call | tf_op jit(solution)/shard_map/layer/pallas_call | solution.py:897
  94.1 2.1 %copy.17 = bf16[192,2048]{1,0:T(8,128)(2,1)} copy(bf16[192,2048]{1,0:T(8,128)(2,1)} %layer.1) | data formatting | bytes 1572864

commit v7 on v6

--- a/solution.py
+++ b/solution.py
@@ -209,18 +209,6 @@
     3 | OTHER | OUT,
     1 | OUT | LATER,
     0 | OUT | LATER,
-    0,
-    0,
-    0,
-    0,
-    0,
-    0,
-    0,
-    0,
-    0,
-    0,
-    0,
-    0,
 )
 INNER_STEPS = (
     4 | OWN | ARRIVE | FORWARD,
@@ -658,166 +646,175 @@
         ref = P.at[at, :, cols]
         remote(ref, ref, sum_s.at[0, m], sum_r.at[at, m], (sp, core_peer)).wait_recv()
 
-    def step(n, carry):
-        code = 0
-        for i, (a, b) in enumerate(zip(OUTER_STEPS, INNER_STEPS)):
-            code = jnp.where(n == i, jnp.where(outer, a, b), code)
-        item = code % 8
-
-        def has(flag):
-            return code // flag % 2 == 1
-
-        slot = item // 2
-        c = item % 2
-
-        @pl.when(has(ARRIVE))
-        def _():
-            forwards = has(FORWARD)
-            across = slot == 0
-            for k in range(2):
-                rows_copy(item, (sp, core_peer), item, item, k).wait_recv()
-
-                @pl.when(forwards)
-                def _():
-                    rows_copy(
-                        item,
-                        (line(jnp.where(across, 2, 0)), tp),
-                        jnp.where(across, 6 + c, item),
-                        jnp.where(across, 10 + c, item),
-                        k,
-                    ).start()
-
-        def specials():
-            @pl.when(has(DOWN_PASS))
+    def run_steps(steps, outer, own):
+        def step(n, carry):
+            code = 0
+            for i, value in enumerate(steps):
+                code = jnp.where(n == i, value, code)
+            item = code % 8
+
+            def has(flag):
+                return code // flag % 2 == 1
+
+            slot = item // 2
+            c = item % 2
+
+            @pl.when(has(ARRIVE))
             def _():
-                for t in early:
-                    tile_on(t, 2, 3)
-
-            @pl.when(has(SEND_ACROSS))
+                forwards = has(FORWARD)
+                across = slot == 0
+                for k in range(2):
+                    rows_copy(item, (sp, core_peer), item, item, k).wait_recv()
+
+                    @pl.when(forwards)
+                    def _():
+                        rows_copy(
+                            item,
+                            (line(jnp.where(across, 2, 0)), tp),
+                            jnp.where(across, 6 + c, item),
+                            jnp.where(across, 10 + c, item),
+                            k,
+                        ).start()
+
+            def specials():
+                @pl.when(has(DOWN_PASS))
+                def _():
+                    for t in early:
+                        tile_on(t, 2, 3)
+
+                @pl.when(has(SEND_ACROSS))
+                def _():
+                    for k in range(2):
+                        send_own(1, k, True)
+
+                @pl.when(has(FIRST_PASS))
+                def _():
+                    weight_on(0, 7, 6)
+                    weight_on(1, 7, 6)
+
+                for k in range(2):
+
+                    @pl.when(has((GATE_PASS, UP_PASS)[k]))
+                    def _():
+                        weight_on(k, 1, 4)
+                        weight_on(k, 2, 5)
+
+                @pl.when(has(DOWN_READY))
+                def _():
+                    for t in early:
+                        tile_copy(t, 1).wait_recv()
+                        tile_copy(t, 3).wait_recv()
+
+                @pl.when(has(FAR_PASS))
+                def _():
+                    down_copy(0).wait_recv()
+                    down_copy(1).wait_recv()
+                    down_copy(2).start()
+                    down_copy(3).start()
+
+                @pl.when(has(HIDDEN_READY))
+                def _():
+                    for k in range(2):
+                        for leg in range(3, 7):
+                            weight_copy(k, leg).wait_recv()
+
+                @pl.when(has(SEND_OUTWARD))
+                def _():
+                    for k in range(2):
+                        send_own(1, k, False)
+
+                @pl.when(has(LATE_RELAY))
+                def _():
+                    for t in late:
+                        tile_on(t, 0, 1, 2)
+
+                @pl.when(has(LATE_PASS))
+                def _():
+                    for t in late:
+                        tile_on(t, 2, 3)
+
+                @pl.when(has(LATE_READY))
+                def _():
+                    for t in late:
+                        tile_copy(t, 1).wait_recv()
+                        tile_copy(t, 3).wait_recv()
+
+                @pl.when(has(FAR_READY))
+                def _():
+                    down_copy(3).wait_recv()
+                    down_copy(4).start()
+                    down_copy(2).wait_recv()
+                    down_copy(4).wait_recv()
+
+            pl.when(code >= SPECIAL)(specials)
+
+            @pl.when(has(OWN))
             def _():
-                for k in range(2):
-                    send_own(1, k, True)
-
-            @pl.when(has(FIRST_PASS))
+                hidden(item, 0)
+
+            @pl.when(has(OTHER))
             def _():
-                weight_on(0, 7, 6)
-                weight_on(1, 7, 6)
-
-            for k in range(2):
-
-                @pl.when(has((GATE_PASS, UP_PASS)[k]))
-                def _():
-                    weight_on(k, 1, 4)
-                    weight_on(k, 2, 5)
-
-            @pl.when(has(DOWN_READY))
+                hidden(item, 1)
+
+            middle = jnp.logical_or(slot == 1, item == 5)
+            begins = code // LATER % 2 == 0
+
+            short = jnp.logical_and(outer, middle)
+
+            @pl.when(jnp.logical_and(has(OUT), short))
             def _():
-                for t in early:
-                    tile_copy(t, 1).wait_recv()
-                    tile_copy(t, 3).wait_recv()
-
-            @pl.when(has(FAR_PASS))
+                hidden_copy(item).start()
+
+            @pl.when(jnp.logical_and(has(OUT), jnp.logical_not(short)))
             def _():
-                down_copy(0).wait_recv()
-                down_copy(1).wait_recv()
-                down_copy(2).start()
-                down_copy(3).start()
-
-            @pl.when(has(HIDDEN_READY))
-            def _():
-                for k in range(2):
-                    for leg in range(3, 7):
-                        weight_copy(k, leg).wait_recv()
-
-            @pl.when(has(SEND_OUTWARD))
-            def _():
-                for k in range(2):
-                    send_own(1, k, False)
-
-            @pl.when(has(LATE_RELAY))
-            def _():
-                for t in late:
-                    tile_on(t, 0, 1, 2)
-
-            @pl.when(has(LATE_PASS))
-            def _():
-                for t in late:
-                    tile_on(t, 2, 3)
-
-            @pl.when(has(LATE_READY))
-            def _():
-                for t in late:
-                    tile_copy(t, 1).wait_recv()
-                    tile_copy(t, 3).wait_recv()
-
-            @pl.when(has(FAR_READY))
-            def _():
-                down_copy(3).wait_recv()
-                down_copy(4).start()
-                down_copy(2).wait_recv()
-                down_copy(4).wait_recv()
-
-        pl.when(code >= SPECIAL)(specials)
-
-        @pl.when(has(OWN))
-        def _():
-            hidden(item, 0)
-
-        @pl.when(has(OTHER))
-        def _():
-            hidden(item, 1)
-
-        middle = jnp.logical_or(slot == 1, item == 5)
-        begins = code // LATER % 2 == 0
-
-        short = jnp.logical_and(outer, middle)
-
-        @pl.when(jnp.logical_and(has(OUT), short))
-        def _():
-            hidden_copy(item).start()
-
-        @pl.when(jnp.logical_and(has(OUT), jnp.logical_not(short)))
-        def _():
-            inner_at = jnp.where(slot == 1, 7 + c, jnp.where(slot == 2, jnp.where(c == 0, 9, 0), 3 + c))
-            a = jnp.where(slot == 0, 5 + c, jnp.where(outer, 0, inner_at))
-            d = jnp.where(slot == own, 1 + c, 0)
-
-            @pl.when(jnp.logical_and(middle, begins))
-            def _():
-                ref = HR.at[held(item)]
-                remote(ref, ref, hid_s.at[0], hid_r.at[held(item)], (sp, core_peer)).wait_recv()
-
-            def some(m, carry):
-                cols = pl.ds(pl.multiple_of(m * tile, tile), tile)
-
-                stage[...] = jnp.dot(H[item], wd[:, cols], preferred_element_type=jnp.float32)
-
-                @pl.when(middle)
-                def _():
-                    stage[...] += jnp.dot(HR[held(item)], wdo[:, cols], preferred_element_type=jnp.float32)
-
-                @pl.when(a > 0)
-                def _():
-                    came(a, m)
-
-                S[item, :, cols] = bf16(stage[...] + f32(P[d, :, cols]) + f32(P[a, :, cols]))
-
-                @pl.when(slot == own)
-                def _():
-                    out_copy(c, m).start()
-
-                @pl.when(slot != own)
-                def _():
-                    sum_copy(item, m).start()
-
-                return carry
-
-            begin = jnp.where(begins, 0, tiles // 2)
-            lax.fori_loop(begin, begin + tiles // 2, some, 0)
-
-        return carry
-
-    lax.fori_loop(0, len(OUTER_STEPS), step, 0)
+                inner_at = jnp.where(slot == 1, 7 + c, jnp.where(slot == 2, jnp.where(c == 0, 9, 0), 3 + c))
+                a = jnp.where(slot == 0, 5 + c, jnp.where(outer, 0, inner_at))
+                d = jnp.where(slot == own, 1 + c, 0)
+
+                @pl.when(jnp.logical_and(middle, begins))
+                def _():
+                    ref = HR.at[held(item)]
+                    remote(ref, ref, hid_s.at[0], hid_r.at[held(item)], (sp, core_peer)).wait_recv()
+
+                def some(m, carry):
+                    cols = pl.ds(pl.multiple_of(m * tile, tile), tile)
+
+                    stage[...] = jnp.dot(H[item], wd[:, cols], preferred_element_type=jnp.float32)
+
+                    @pl.when(middle)
+                    def _():
+                        stage[...] += jnp.dot(HR[held(item)], wdo[:, cols], preferred_element_type=jnp.float32)
+
+                    @pl.when(a > 0)
+                    def _():
+                        came(a, m)
+
+                    S[item, :, cols] = bf16(stage[...] + f32(P[d, :, cols]) + f32(P[a, :, cols]))
+
+                    @pl.when(slot == own)
+                    def _():
+                        out_copy(c, m).start()
+
+                    @pl.when(slot != own)
+                    def _():
+                        sum_copy(item, m).start()
+
+                    return carry
+
+                begin = jnp.where(begins, 0, tiles // 2)
+                lax.fori_loop(begin, begin + tiles // 2, some, 0)
+
+            return carry
+
+        lax.fori_loop(0, len(steps), step, 0)
+
+    @pl.when(outer)
+    def _():
+        run_steps(OUTER_STEPS, True, 0)
+
+    @pl.when(inner)
+    def _():
+        run_steps(INNER_STEPS, False, 1)
 
     for c in range(2):
         for m in range(depth // tile):

time: 96.8 us -> 96.7 us (level)
  no operation moved by 1% of the time
where the time goes in v7:
time: 96.7 us; the launch traced here: 96.2 us
  Pallas kernels  94.1 us (97%)
  local copies, waits for them, and re-layouts  2.09 us (2%)
    pallas_call x1, Pallas kernels, mega(): pl.pallas_call(mega_kernel, out_shape=jax.ShapeDtypeStruct((rows, depth),...  94.1 us
    unnamed x1, local copies, waits for them, and re-layouts  2.09 us

profile of v7, /device:TPU:12, one launch (start us, length us, event | category | flops | bytes accessed | tf_op | source)
XLA Modules:
  0.0 96.2 jit_solution(11583894745597183202)
XLA Ops:
  0.0 94.1 %layer.1 = bf16[192,2048]{1,0:T(8,128)(2,1)} custom-call(bf16[768,512]{1,0:T(8,128)(2,1)} %co_hbm.1, bf16[768,512]{1,0:T(8,128)(2,1)} %ci_hbm.1, bf16[768,512]{1,0:T(8,128)(2,1)} %cx_hbm.1, f32[3,512]{1,0:T(4,128)} %taps.1, bf16[512,2048]{1,0:T(8,128)(2,1)} %ow_hbm.1, bf16[192,2048]{1,0:T(8,128)(2,1)} %mg_hbm.1, bf16[192,2048]{1,0:T(8,128)(2,1)} %res_hbm.1, ...), custom_call_target="tpu_custom_call" | custom-call | tf_op jit(solution)/shard_map/layer/pallas_call | solution.py:894
  94.1 2.1 %copy.17 = bf16[192,2048]{1,0:T(8,128)(2,1)} copy(bf16[192,2048]{1,0:T(8,128)(2,1)} %layer.1) | data formatting | bytes 1572864
